TPU v7x, 512 devices: a whole 4x8x8 slice. The times are simulated.
512 devices in a mesh: kv: 64 (over z, y), tp: 8 (over x, core).
Axes of the slice: x: 4, y: 8, z: 8, core: 2. Of those that a mesh axis runs over, the one named last changes fastest.
Arguments:
- tokens: bfloat16 [256, 4, 2048], P('kv', None, 'tp'), may hold values from -6 to 6
- input_gain: float32 [2048], replicated, may hold values from 0.1 to 1.9
- gate_weight: bfloat16 [2048, 4096], P('kv', 'tp'), may hold values from -0.125 to 0.125
- value_weight: bfloat16 [2048, 4096], P('kv', 'tp'), may hold values from -0.125 to 0.125
- write_weight: bfloat16 [2048, 1024], P('kv', 'tp'), may hold values from -0.125 to 0.125
- read_weight: bfloat16 [2048, 1024], P('kv', 'tp'), may hold values from -0.125 to 0.125
- step_weight: bfloat16 [2048, 64], replicated, may hold values from -0.125 to 0.125
- conv_value: float32 [4, 4096], P(None, 'tp'), may hold values from -3 to 3
- conv_write: float32 [4, 1024], P(None, 'tp'), may hold values from -3 to 3
- conv_read: float32 [4, 1024], P(None, 'tp'), may hold values from -3 to 3
- step_bias: float32 [64], P('tp'), may hold values from -4 to -1
- decay_log: float32 [64], P('tp'), may hold values from 0 to 2.8
- skip_gain: float32 [64], P('tp'), may hold values from 0.5 to 1.5
- output_gain: float32 [4096], P('tp'), may hold values from 0.1 to 1.9
- out_weight: bfloat16 [4096, 2048], P('tp', 'kv'), may hold values from -0.09375 to 0.09375
- base_state: float32 [256, 64, 64, 128], P('kv', 'tp'), may hold values from -2 to 2
- past_value: bfloat16 [256, 7, 4096], P('kv', None, 'tp'), may hold values from -6 to 6
- past_write: bfloat16 [256, 7, 1024], P('kv', None, 'tp'), may hold values from -6 to 6
- past_read: bfloat16 [256, 7, 1024], P('kv', None, 'tp'), may hold values from -6 to 6
- past_step: bfloat16 [256, 4, 64], P('kv', None, 'tp'), may hold values from -4 to 4
- accepted: int32 [256], P('kv'), may hold values from 1 to 4
Outputs:
- mixed: bfloat16 [256, 4, 2048], P('kv', None, 'tp')
- root_state: float32 [256, 64, 64, 128], P('kv', 'tp')
- next_value: bfloat16 [256, 7, 4096], P('kv', None, 'tp')
- next_write: bfloat16 [256, 7, 1024], P('kv', None, 'tp')
- next_read: bfloat16 [256, 7, 1024], P('kv', None, 'tp')
- next_step: bfloat16 [256, 4, 64], P('kv', None, 'tp')
Inputs may be any that keep to these rules, and one draw needn't show every extreme that they name: Every entry of `accepted` is an integer from 1 to 4 (at least one of the last step's proposals is always accepted).
All inputs are finite; a program needn't handle non-finite values.
Results may differ from a plain program's by a relative error of at most 0.018.
Values may be sent and summed in bfloat16 or wider, within the bound.
A program may use at most 64 MiB of HBM per device.

v0:
```python
import jax
import jax.numpy as jnp
from jax import lax
from jax.sharding import PartitionSpec as P

STATE_DIM = 128
CONV_W = 4


EPSILON = 1e-06


def sent_together(arrays, axis, dim, along):
    ends, at = ([], 0)
    for a in arrays[:-1]:
        at += a.shape[along]
        ends.append(at)
    both = jnp.concatenate(arrays, axis=along)
    return tuple(jnp.split(lax.all_gather(both, axis, axis=dim, tiled=True), ends, axis=along))


def split_up(value, dim, peers):
    before, after = (value.shape[:dim], value.shape[dim + 1 :])
    return jnp.moveaxis(value.reshape(*before, peers, -1, *after), dim, 0)


def summed_on_arrival(value, axis, dim):
    pieces = split_up(value, dim, lax.axis_size(axis))
    arrived = lax.all_to_all(pieces, axis, split_axis=0, concat_axis=0, tiled=True)
    return arrived.astype(jnp.float32).sum(axis=0)


def causal_conv(rows, kernel):
    width = kernel.shape[0]
    count = rows.shape[0] - width + 1
    total = kernel[0] * rows[0:count]
    for offset in range(1, width):
        total = total + kernel[offset] * rows[offset : offset + count]
    return total


def advance(
    past_x,
    past_b,
    past_c,
    past_dt,
    taken,
    state_zero,
    value_now,
    write_now,
    read_now,
    gate_now,
    step_now,
    conv_value,
    conv_write,
    conv_read,
    step_bias,
    decay_log,
    skip_gain,
    output_gain,
):
    highest = lax.Precision.HIGHEST
    proposals = value_now.shape[0]
    head_count = step_bias.shape[0]
    group_count = write_now.shape[1] // STATE_DIM
    per_group = head_count // group_count
    head_width = value_now.shape[1] // head_count
    rate = jnp.exp(decay_log)
    prev_x = jax.nn.silu(causal_conv(past_x.astype(jnp.float32), conv_value)).reshape(
        proposals, head_count, head_width
    )
    prev_b = jax.nn.silu(causal_conv(past_b.astype(jnp.float32), conv_write)).reshape(
        proposals, group_count, STATE_DIM
    )
    prev_b = jnp.repeat(prev_b, per_group, axis=1)
    prev_dt = jax.nn.softplus(past_dt.astype(jnp.float32) + step_bias)
    live = (jnp.arange(proposals, dtype=jnp.int32) < taken)[:, None]
    prev_log = jnp.where(live, -rate * prev_dt, jnp.zeros_like(prev_dt))
    total_log = jnp.sum(prev_log, axis=0)
    tail_log = total_log - jnp.cumsum(prev_log, axis=0)
    weight_now = jnp.where(live, jnp.exp(tail_log) * prev_dt, jnp.zeros_like(prev_dt))
    root = jnp.exp(total_log)[:, None, None] * state_zero + jnp.einsum(
        "sh,shp,shn->hpn", weight_now, prev_x, prev_b, precision=highest
    )
    window_x = jnp.concatenate(
        [lax.dynamic_slice_in_dim(past_x, taken, CONV_W - 1, 0), value_now], axis=0
    )
    window_b = jnp.concatenate(
        [lax.dynamic_slice_in_dim(past_b, taken, CONV_W - 1, 0), write_now], axis=0
    )
    window_c = jnp.concatenate(
        [lax.dynamic_slice_in_dim(past_c, taken, CONV_W - 1, 0), read_now], axis=0
    )
    cur_x = jax.nn.silu(causal_conv(window_x.astype(jnp.float32), conv_value)).reshape(
        proposals, head_count, head_width
    )
    cur_b = jax.nn.silu(causal_conv(window_b.astype(jnp.float32), conv_write)).reshape(
        proposals, group_count, STATE_DIM
    )
    cur_c = jax.nn.silu(causal_conv(window_c.astype(jnp.float32), conv_read)).reshape(
        proposals, group_count, STATE_DIM
    )
    cur_b = jnp.repeat(cur_b, per_group, axis=1)
    cur_c = jnp.repeat(cur_c, per_group, axis=1)
    cur_dt = jax.nn.softplus(step_now.astype(jnp.float32) + step_bias)
    logs = jnp.cumsum(-rate * cur_dt, axis=0)
    carried = jnp.einsum("thn,hpn->thp", cur_c, root, precision=highest) * jnp.exp(logs)[:, :, None]
    lower = (jnp.arange(proposals)[:, None] >= jnp.arange(proposals)[None, :])[:, :, None]
    diff = logs[:, None, :] - logs[None, :, :]
    decay = jnp.where(
        lower, jnp.exp(jnp.where(lower, diff, jnp.zeros_like(diff))), jnp.zeros_like(diff)
    )
    scores = (
        jnp.einsum("thn,shn->tsh", cur_c, cur_b, precision=highest) * decay * cur_dt[None, :, :]
    )
    inner = jnp.einsum("tsh,shp->thp", scores, cur_x, precision=highest)
    mixed = carried + inner + skip_gain[None, :, None] * cur_x
    gated = mixed.reshape(proposals, -1) * jax.nn.silu(gate_now.astype(jnp.float32))
    grouped = gated.reshape(proposals, group_count, -1)
    grouped = grouped * lax.rsqrt(jnp.mean(grouped * grouped, axis=-1, keepdims=True) + EPSILON)
    result = (grouped.reshape(proposals, -1) * output_gain).astype(jnp.bfloat16)
    return (result, root, window_x, window_b, window_c)


def on_device(
    tokens,
    input_gain,
    gate_weight,
    value_weight,
    write_weight,
    read_weight,
    step_weight,
    conv_value,
    conv_write,
    conv_read,
    step_bias,
    decay_log,
    skip_gain,
    output_gain,
    out_weight,
    base_state,
    past_value,
    past_write,
    past_read,
    past_step,
    accepted,
):
    whole = lax.all_gather(tokens, "tp", axis=2, tiled=True)
    seq_local, proposals, width = whole.shape
    rows = whole.astype(jnp.float32)
    normed = (
        rows * lax.rsqrt(jnp.mean(rows * rows, axis=-1, keepdims=True) + EPSILON) * input_gain
    ).astype(jnp.bfloat16)
    flat = normed.reshape(seq_local * proposals, width)
    token_count = flat.shape[0]
    head_count = step_bias.shape[0]
    own_step = lax.dynamic_slice_in_dim(
        step_weight, lax.axis_index("tp") * head_count, head_count, 1
    )
    step_now = jnp.dot(flat, own_step, preferred_element_type=jnp.float32).astype(jnp.bfloat16)
    pieces = sent_together((gate_weight, value_weight, write_weight, read_weight), "kv", 0, 1)
    gate_sum, value_sum, write_sum, read_sum = tuple(
        (jnp.dot(flat, piece, preferred_element_type=jnp.float32) for piece in pieces)
    )
    gate_now = gate_sum.astype(jnp.bfloat16)
    value_now = value_sum.astype(jnp.bfloat16)
    write_now = write_sum.astype(jnp.bfloat16)
    read_now = read_sum.astype(jnp.bfloat16)
    shaped = [
        item.reshape(seq_local, proposals, item.shape[1])
        for item in (value_now, write_now, read_now, gate_now, step_now)
    ]
    stepper = jax.vmap(advance, in_axes=(0,) * 11 + (None,) * 7)
    normal_out, root_state, next_value, next_write, next_read = stepper(
        past_value,
        past_write,
        past_read,
        past_step,
        accepted,
        base_state,
        shaped[0],
        shaped[1],
        shaped[2],
        shaped[3],
        shaped[4],
        conv_value,
        conv_write,
        conv_read,
        step_bias,
        decay_log,
        skip_gain,
        output_gain,
    )
    flat_y = normal_out.reshape(token_count, -1)
    partial_sum = jnp.dot(
        flat_y,
        lax.all_gather(out_weight, "kv", axis=1, tiled=True),
        preferred_element_type=jnp.float32,
    )
    summed = summed_on_arrival(partial_sum.astype(jnp.bfloat16), "tp", 1)
    mixed = summed.astype(jnp.bfloat16).reshape(seq_local, proposals, summed.shape[1])
    return (mixed, root_state, next_value, next_write, next_read, shaped[4])


def solution(mesh):
    return jax.shard_map(
        on_device,
        mesh=mesh,
        in_specs=(
            P("kv", None, "tp"),
            P(),
            P("kv", "tp"),
            P("kv", "tp"),
            P("kv", "tp"),
            P("kv", "tp"),
            P(),
            P(None, "tp"),
            P(None, "tp"),
            P(None, "tp"),
            P("tp"),
            P("tp"),
            P("tp"),
            P("tp"),
            P("tp", "kv"),
            P("kv", "tp", None, None),
            P("kv", None, "tp"),
            P("kv", None, "tp"),
            P("kv", None, "tp"),
            P("kv", None, "tp"),
            P("kv"),
        ),
        out_specs=(
            P("kv", None, "tp"),
            P("kv", "tp", None, None),
            P("kv", None, "tp"),
            P("kv", None, "tp"),
            P("kv", None, "tp"),
            P("kv", None, "tp"),
        ),
        check_vma=False,
    )
```

profile of v0, /device:TPU:1, one launch (start us, length us, event | category | flops | bytes accessed | tf_op | source)
XLA Modules:
  0.0 207.6 jit_solution(918326364809412777)
XLA Ops:
  7.2 0.0 copy-start
  7.2 0.0 copy-start.2
  7.2 0.0 all-gather.3.cloned.1.call-start
  7.2 1.5 pad_maximum_fusion
  8.8 0.0 all-gather.3.cloned.1.call-update
  8.8 0.0 all-gather.5.cloned.1.call-start
  8.9 0.7 all-gather.5.cloned.1.call-update
  9.6 0.7 fusion.52
  10.2 0.7 iota_compare_fusion.1
  11.0 0.7 convert_element_type.70
  11.7 1.3 gather_fusion.2
  13.0 1.4 gather_fusion.1
  14.3 0.8 convert_element_type.69
  15.1 18.1 %all_gather.9 = bf16[4,4,2048]{2,1,0:T(4,128)(2,1)S(1)} all-gather(bf16[4,4,256]{2,1,0:T(4,128)(2,1)} %param.21), channel_id=1, replica_groups=mesh['kv'=64,'tp'=8] {'tp'}, dimensions={2}, use_global_device_ids=true | all-gather | bytes 73728 | tf_op jit(solution)/shard_map/all_gather | solution.py:148
  33.2 0.1 fusion.17
  33.3 0.8 fusion.19
  34.1 0.0 copy-done
  34.1 0.1 convolution_convert_fusion.3
  34.3 0.1 copy.86
  34.4 0.0 copy-start.4
  34.4 0.7 exponential_negate_fusion
  35.0 0.8 fusion.56
  35.9 0.1 copy.91
  36.0 1.3 gather_fusion
  37.3 0.8 slice_bitcast_fusion.7
  38.2 0.8 multiply_select_fusion
  39.0 0.1 copy.80
  39.1 0.1 copy.93
  39.2 0.8 slice_bitcast_fusion.3
  40.0 0.9 fusion.57
  40.9 0.0 copy-start.8
  40.9 60.4 %all-gather.3.cloned.1.call-done = bf16[2048,1280]{1,0:T(8,128)(2,1)} async-done(((bf16[32,1280]{1,0:T(8,128)(2,1)}), bf16[2048,1280]{1,0:T(8,128)(2,1)}) %all-gather.3.cloned.1.call-update) | async-done | bytes 5242896 | tf_op jit(solution)/shard_map/all_gather | solution.py:19
  101.3 1.2 convolution_convert_fusion.2
  102.5 0.0 copy-start.7
  102.5 1.2 convolution_convert_fusion.1
  103.8 0.0 copy-start.5
  103.8 0.0 copy-start.6
  103.9 2.0 fusion.6
  105.9 0.0 copy-start.3
  105.9 0.1 divide_multiply_fusion.1
  106.0 0.1 reshape.160
  106.2 0.1 reshape.167
  106.3 2.0 fusion.12
  108.2 0.1 reshape.173
  108.3 0.4 fusion.5
  108.7 0.4 fusion.21
  109.1 0.0 copy-done.2
  109.1 1.9 convolution_add_fusion
  111.0 0.0 copy-start.1
  111.1 1.7 fusion.34
  112.8 0.0 copy-done.4
  112.8 0.0 copy-done.8
  112.8 0.2 multiply_reduce_fusion
  113.0 0.1 reshape.170
  113.1 0.1 rsqrt.21
  113.2 70.7 %all-gather.5.cloned.1.call-done = bf16[512,2048]{0,1:T(8,128)(2,1)} async-done(((bf16[512,32]{0,1:T(8,128)(2,1)}), bf16[512,2048]{0,1:T(8,128)(2,1)}) %all-gather.5.cloned.1.call-update) | async-done | bytes 2097168 | tf_op jit(solution)/shard_map/all_gather | solution.py:197
  183.9 0.0 copy-done.7
  183.9 2.2 %convolution_convert_fusion = bf16[16,2048]{1,0:T(8,128)(2,1)S(1)} fusion(bf16[512,2048]{0,1:T(8,128)(2,1)} %all-gather.5.cloned.1.call-done, f32[16,512]{1,0:T(8,128)S(1)} %reshape.170, f32[16,512]{1,0:T(8,128)S(1)} %fusion.12, f32[512]{0:T(512)S(1)} %copy-done.7, f32[16]{0:T(128)S(1)} %rsqrt.21), kind=kOutput, calls=%fused_computation.3 | convolution fusion | flops 33652736 | bytes 2230336 | tf_op jit(solution)/shard_map/dot_general | solution.py:195
  186.1 0.0 copy-done.5
  186.1 0.0 copy-done.6
  186.2 13.9 %all_to_all.5 = bf16[8,16,256]{2,1,0:T(8,128)(2,1)S(1)} all-to-all(bf16[8,16,256]{2,1,0:T(8,128)(2,1)S(1)} %bitcast.67), channel_id=1, replica_groups=mesh['kv'=64,'tp'=8] {'tp'}, dimensions={0} | all-to-all | bytes 131072 | tf_op jit(solution)/shard_map/all_to_all | solution.py:29
  200.1 0.6 reshape.172
  200.7 0.0 copy-done.3
  200.7 0.0 copy-done.1
  (25 shorter events, 0.3 us)
Async XLA Ops:
  7.2 27.0 %copy-start = (bf16[2048,64]{0,1:T(8,128)(2,1)S(1)}, bf16[2048,64]{0,1:T(8,128)(2,1)}, u32[]{:S(2)}) copy-start(bf16[2048,64]{0,1:T(8,128)(2,1)} %param.27) | copy-start | bytes 786436
  7.2 101.9 %copy-start.2 = (f32[4,8,64,128]{3,2,1,0:T(8,128)S(1)}, f32[4,8,64,128]{3,2,1,0:T(8,128)}, u32[]{:S(2)}) copy-start(f32[4,8,64,128]{3,2,1,0:T(8,128)} %param.36) | copy-start | bytes 3145732
  7.2 94.1 %all-gather.3.cloned.1.call-start = ((), (), s32[]{:S(2)}) async-start(), calls=%async_computation.1 | async-start | bytes 5324800 | tf_op jit(solution)/shard_map/all_gather | solution.py:19
  8.8 175.1 %all-gather.5.cloned.1.call-start = ((), (), s32[]{:S(2)}) async-start(), calls=%async_computation.2 | async-start | bytes 2129920 | tf_op jit(solution)/shard_map/all_gather | solution.py:197
  34.4 78.4 %copy-start.4 = (bf16[16,8]{1,0:T(8,128)(2,1)}, bf16[16,8]{1,0:T(8,128)(2,1)S(1)}, u32[]{:S(2)}) copy-start(bf16[16,8]{1,0:T(8,128)(2,1)S(1)} %copy.86) | copy-start | bytes 772
  40.9 71.9 %copy-start.8 = (f32[8]{0:T(128)S(1)}, f32[8]{0:T(128)}, u32[]{:S(2)}) copy-start(f32[8]{0:T(128)} %param.33) | copy-start | bytes 100
  102.5 81.4 %copy-start.7 = (f32[512]{0:T(512)S(1)}, f32[512]{0:T(512)}, u32[]{:S(2)}) copy-start(f32[512]{0:T(512)} %param.34) | copy-start | bytes 6148
  103.8 82.4 %copy-start.5 = (bf16[4,7,128]{2,0,1:T(4,128)(2,1)}, bf16[4,7,128]{2,0,1:T(4,128)(2,1)S(1)}, u32[]{:S(2)}) copy-start(bf16[4,7,128]{2,0,1:T(4,128)(2,1)S(1)} %get-tuple-element.30) | copy-start | bytes 21508
  103.8 82.4 %copy-start.6 = (bf16[4,7,128]{2,0,1:T(4,128)(2,1)}, bf16[4,7,128]{2,0,1:T(4,128)(2,1)S(1)}, u32[]{:S(2)}) copy-start(bf16[4,7,128]{2,0,1:T(4,128)(2,1)S(1)} %get-tuple-element.31) | copy-start | bytes 21508
  105.9 94.8 %copy-start.3 = (bf16[4,7,512]{2,0,1:T(4,128)(2,1)}, bf16[4,7,512]{2,0,1:T(4,128)(2,1)S(1)}, u32[]{:S(2)}) copy-start(bf16[4,7,512]{2,0,1:T(4,128)(2,1)S(1)} %copy_dynamic-update-slice_fusion) | copy-start | bytes 86020
  111.0 89.7 %copy-start.1 = (f32[4,8,64,128]{3,2,1,0:T(8,128)}, f32[4,8,64,128]{3,2,1,0:T(8,128)S(1)}, u32[]{:S(2)}) copy-start(f32[4,8,64,128]{3,2,1,0:T(8,128)S(1)} %convolution_add_fusion) | copy-start | bytes 3145732
Sparse Core Ops, SparseCore 0:
  11.6 89.6 all-gather.2
  104.4 79.4 all-gather.4
where the time goes:
time: 208 us
  waiting for transfers between devices  132 us (63%)
  blocking collectives  32 us (15%)
  between operations  14.3 us (7%)
  matrix products  13.2 us (6%)
  local copies, waits for them, and re-layouts  8.14 us (4%)
  other arithmetic  8.01 us (4%)
    all_gather x1, waiting for transfers between devices, on_device(): lax.all_gather(out_weight, 'kv', axis=1, tiled=True)  70.7 us
    all_gather x1, waiting for transfers between devices, sent_together(): lax.all_gather(both, axis, axis=dim, tiled=True)  60.4 us
    all_gather x1, blocking collectives, on_device(): whole = lax.all_gather(tokens, 'tp', axis=2, tiled=True)  18.1 us
    all_to_all x1, blocking collectives, summed_on_arrival(): lax.all_to_all(pieces, axis, split_axis=0, concat_axis=0, tiled=True)  13.9 us
    dot_general x4, matrix products, on_device(): jnp.dot(flat, piece, preferred_element_type=jnp.float32)  6.38 us
  transfers between devices with their start and end apart: 2, of which 2 were waited for; matrix products, arithmetic and copies ran while one was open for 12% of the time, Pallas kernels for 0%

commit v1 on v0

v1 whole, which is shorter than its diff:
```python
import jax
import jax.numpy as jnp
from jax import lax
from jax.experimental import pallas as pl
from jax.experimental.pallas import tpu as pltpu
from jax.sharding import PartitionSpec as P

F32 = jnp.float32
BF16 = jnp.bfloat16
MESH = pl.DeviceIdType.MESH
EPSILON = 1e-06
HIGHEST = lax.Precision.HIGHEST

N = 8
SEQ = 4
PROP = 4
ROWS = SEQ * PROP
CONV = 4
PAST = 7
NT = (((1,), (1,)), ((), ()))
TN = (((0,), (0,)), ((), ()))
FAR = (4, 3, 5)
NEAR = (2, 6, 1, 7)

T1, T2Y, T2Z, WY, WZ, RSY, RSZ, OW, O1, O2 = range(10)


def silu(v):
    return v / (1.0 + jnp.exp(-v))


def softplus(v):
    return jnp.maximum(v, 0.0) + jnp.log1p(jnp.exp(-jnp.abs(v)))


def conv(buf, taps, at=0):
    total = taps[0:1, :] * buf[at : at + ROWS, :]
    for k in range(1, CONV):
        total = total + taps[k : k + 1, :] * buf[at + SEQ * k : at + SEQ * k + ROWS, :]
    return total


def body(
    tokens, input_gain, gate_w, value_w, write_w, read_w, step_w,
    conv_v, conv_b, conv_c, step_bias, decay_log, skip_gain, output_gain,
    out_w, base, past_v, past_b, past_c, past_s, accepted,
    mixed_o, root_o, nv_o, nb_o, nc_o, ns_o,
    gain_m, stepw_m, cv_m, cb_m, cc_m, bias_m, decay_m, skip_m, og_m,
    base_m, pv_m, pb_m, pc_m, ps_m,
    xall, nrm, npk, ay, az, wy, wz, py, pz, rsy, rsz, owg, nrg, po, osum,
    xf, ppv, ppb, ppc, rrv, rrb, rrc, stp, sbuf, ubuf, bbuf, xb, bb, lb, dtb, dj, rootb, mf, nsf,
    mixed_m, root_m, nv_m, nb_m, nc_m, ns_m,
    in_sem, out_sem, send_sem, recv_sem,
):
    kv = lax.axis_index("kv")
    tp = lax.axis_index("tp")
    z = kv // N
    y = kv % N

    def at(rows, count):
        return pl.ds(pl.multiple_of(rows * count, count), count)

    ins = [
        (value_w, wy.at[at(y, 32), pl.ds(0, 512)]),
        (write_w, wy.at[at(y, 32), pl.ds(512, 128)]),
        (gate_w, wz.at[at(z, 32), pl.ds(0, 512)]),
        (read_w, wz.at[at(z, 32), pl.ds(512, 128)]),
        (out_w, owg.at[at(y, 32), :]),
        (tokens, xall.at[tp]),
        (input_gain, gain_m),
        (past_v, pv_m),
        (past_b, pb_m),
        (past_c, pc_m),
        (past_s, ps_m),
        (conv_v, cv_m),
        (conv_b, cb_m),
        (conv_c, cc_m),
        (step_bias, bias_m),
        (decay_log, decay_m),
        (skip_gain, skip_m),
        (output_gain, og_m),
        (step_w, stepw_m),
        (base, base_m),
    ]
    loads = [pltpu.make_async_copy(s, d, in_sem.at[i]) for i, (s, d) in enumerate(ins)]
    for c in loads:
        c.start()

    barrier = pltpu.get_barrier_semaphore()

    def tell(k, t):
        pl.semaphore_signal(barrier, inc=1, device_id=(k, t), device_id_type=MESH)

    for d in range(1, N):
        tell(kv, (tp + d) % N)
        tell(z * N + (y + d) % N, tp)
        tell(((z + d) % N) * N + y, tp)
        tell(tp * N + y, (tp + d) % N)

    @pl.when(z != tp)
    def _():
        tell(tp * N + y, tp)

    for c in loads[:6]:
        c.wait()
    pl.semaphore_wait(barrier, 4 * (N - 1) + jnp.where(z != tp, 1, 0).astype(jnp.int32))

    sent = []

    def send(phase, d, src, dst, slot, k, t):
        c = pltpu.make_async_remote_copy(
            src_ref=src, dst_ref=dst, send_sem=send_sem.at[phase, d],
            recv_sem=recv_sem.at[phase, slot], device_id=(k, t), device_id_type=MESH,
        )
        c.start()
        sent.append(c)

    def arrived(phase, slot, ref):
        pltpu.make_async_remote_copy(
            src_ref=ref, dst_ref=ref, send_sem=send_sem.at[phase, 0],
            recv_sem=recv_sem.at[phase, slot], device_id=(kv, tp), device_id_type=MESH,
        ).wait_recv()

    def up(d):
        return z * N + (y + d) % N

    def over(d):
        return ((z + d) % N) * N + y

    def weights(ds):
        for d in ds:
            send(WY, d, wy.at[at(y, 32), :], wy.at[at(y, 32), :], y, up(d), tp)
            send(WZ, d, wz.at[at(z, 32), :], wz.at[at(z, 32), :], z, over(d), tp)

    for d in range(1, N):
        send(T1, d, xall.at[tp], xall.at[tp], tp, kv, (tp + d) % N)
    weights(FAR)

    for c in loads[6:]:
        c.wait()
    for r in range(PAST):
        ppv[SEQ * r : SEQ * r + SEQ, :] = pv_m[r].astype(F32)
        ppb[SEQ * r : SEQ * r + SEQ, :] = pb_m[r].astype(F32)
        ppc[SEQ * r : SEQ * r + SEQ, :] = pc_m[r].astype(F32)

    for d in range(1, N):
        t = (tp + d) % N
        arrived(T1, t, xall.at[t])
    for t in range(N):
        for q in range(SEQ):
            xf[PROP * q : PROP * q + PROP, 256 * t : 256 * t + 256] = xall[t, q].astype(F32)
    rows = xf[...]
    scale = lax.rsqrt(jnp.mean(rows * rows, axis=-1, keepdims=True) + EPSILON)
    normed16 = (rows * scale * gain_m[...]).astype(BF16)
    to = lax.broadcasted_iota(jnp.int32, (ROWS, ROWS), 0)
    by = lax.broadcasted_iota(jnp.int32, (ROWS, ROWS), 1)
    swap = jnp.where((to % SEQ) * PROP + to // SEQ == by, 1.0, 0.0).astype(BF16)
    normed = jnp.dot(swap, normed16, preferred_element_type=F32)
    normed16 = normed.astype(BF16)
    for zz in range(N):
        nrm[zz] = normed16[:, 256 * zz : 256 * zz + 256]
    lane = lax.broadcasted_iota(jnp.int32, (ROWS, 128), 1) // 32
    for yy in range(N):
        for half in range(2):
            tile = None
            for i in range(4):
                start = 256 * (4 * half + i) + 128 * (yy // 4)
                shift = (32 * i - 32 * (yy % 4)) % 128
                piece = normed[:, start : start + 128]
                if shift:
                    piece = pltpu.roll(piece, shift, 1)
                tile = piece if tile is None else jnp.where(lane == i, piece, tile)
            npk[yy, :, 128 * half : 128 * half + 128] = tile.astype(BF16)
    ay[at(z, ROWS), :] = nrm[z]
    az[at(y, ROWS), :] = npk[y]
    for d in FAR + NEAR:
        zz, yy = (z + d) % N, (y + d) % N
        send(T2Y, d, nrm.at[zz], ay.at[at(z, ROWS), :], z, over(d), tp)
        send(T2Z, d, npk.at[yy], az.at[at(y, ROWS), :], y, up(d), tp)
    weights(NEAR)

    head = lax.broadcasted_iota(jnp.int32, (1, 512), 1) // 64

    def spread(ref):
        row = jnp.zeros((1, 512), F32)
        for h in range(8):
            row = jnp.where(head == h, ref[0:1, h : h + 1], row)
        return row

    bias = spread(bias_m)
    rate = jnp.exp(spread(decay_m))
    skip = spread(skip_m)
    step16 = lax.dot_general(normed16, stepw_m[...], NT, preferred_element_type=F32).astype(BF16)
    row64 = lax.broadcasted_iota(jnp.int32, (64, 512), 0)
    own64 = (row64 - 8 * tp == lax.broadcasted_iota(jnp.int32, (64, 512), 1) // 64)
    wide = jnp.dot(step16, jnp.where(own64, 1.0, 0.0).astype(BF16), preferred_element_type=F32)
    row64 = lax.broadcasted_iota(jnp.int32, (64, 128), 0)
    pick = (row64 - 8 * tp == lax.broadcasted_iota(jnp.int32, (64, 128), 1))
    nsf[...] = jnp.dot(step16, jnp.where(pick, 1.0, 0.0).astype(BF16), preferred_element_type=F32)
    for q in range(SEQ):
        ns_m[q] = nsf[pl.ds(q, PROP, stride=SEQ), :][:, 0:8].astype(BF16)

    dt = softplus(wide + bias)
    sbuf[...] = -rate * dt
    run = jnp.zeros((SEQ, 512), F32)
    lb[0:12, :] = jnp.zeros((12, 512), F32)
    dtb[0:12, :] = jnp.zeros((12, 512), F32)
    xb[0:12, :] = jnp.zeros((12, 512), F32)
    bb[0:12, :] = jnp.zeros((12, 128), F32)
    for t in range(PROP):
        run = run + sbuf[SEQ * t : SEQ * t + SEQ, :]
        lb[12 + SEQ * t : 16 + SEQ * t, :] = run
    dtb[12:28, :] = dt
    logs = lb[12:28, :]
    for j in range(PROP):
        lo = 12 - SEQ * j
        dj[j] = jnp.exp(logs - lb[lo : lo + ROWS, :]) * dtb[lo : lo + ROWS, :]

    eight = (
        lax.broadcasted_iota(jnp.int32, (8, 512), 0)
        == lax.broadcasted_iota(jnp.int32, (8, 512), 1) // 64
    )
    eight = jnp.where(eight, 1.0, 0.0).astype(BF16)
    for q in range(SEQ):
        stp[PROP * q : PROP * q + PROP, :] = jnp.dot(
            ps_m[q], eight, preferred_element_type=F32
        )
    steps = jnp.dot(swap, stp[...].astype(BF16), preferred_element_type=F32)
    pd = softplus(steps + bias)

    def taken(shape):
        seq = lax.broadcasted_iota(jnp.int32, shape, 0) % SEQ
        count = jnp.full(shape, accepted[0], jnp.int32)
        for q in range(1, SEQ):
            count = jnp.where(seq == q, accepted[q], count)
        return count

    live = lax.broadcasted_iota(jnp.int32, (ROWS, 512), 0) // SEQ < taken((ROWS, 512))
    sbuf[...] = jnp.where(live, -rate * pd, 0.0)
    pls = [sbuf[SEQ * s : SEQ * s + SEQ, :] for s in range(PROP)]
    tails = [None] * PROP
    run = jnp.zeros((SEQ, 512), F32)
    for s in reversed(range(PROP)):
        tails[s] = run
        run = run + pls[s]
    kept = jnp.exp(run)
    for s in range(PROP):
        stp[SEQ * s : SEQ * s + SEQ, :] = jnp.exp(tails[s])
    ubuf[...] = jnp.where(live, stp[...] * pd, 0.0) * silu(conv(ppv, cv_m))
    bbuf[...] = silu(conv(ppb, cb_m))

    def window(pp, rr, width):
        count = taken((12, width))
        first = pp[SEQ : SEQ + 12, :]
        for a in range(2, PROP + 1):
            first = jnp.where(count == a, pp[SEQ * a : SEQ * a + 12, :], first)
        rr[0:12, :] = first

    window(ppv, rrv, 512)
    window(ppb, rrb, 128)
    window(ppc, rrc, 128)

    for d in range(1, N):
        zz, yy = (z + d) % N, (y + d) % N
        arrived(T2Y, zz, ay.at[at(zz, ROWS), :])
        arrived(T2Z, yy, az.at[at(yy, ROWS), :])
    for d in FAR + NEAR:
        yy = (y + d) % N
        arrived(WY, yy, wy.at[at(yy, 32), :])
    py[...] = jnp.dot(ay[...], wy[...], preferred_element_type=F32).astype(BF16)
    for d in FAR + NEAR:
        zz = (z + d) % N
        arrived(WZ, zz, wz.at[at(zz, 32), :])
    pz[...] = jnp.dot(az[...], wz[...], preferred_element_type=F32).astype(BF16)
    for d in FAR + NEAR:
        zz, yy = (z + d) % N, (y + d) % N
        send(RSY, d, py.at[at(zz, ROWS), :], rsy.at[z], z, over(d), tp)
        send(RSZ, d, pz.at[at(yy, ROWS), :], rsz.at[y], y, up(d), tp)
    for d in FAR + NEAR:
        send(OW, d, owg.at[at(y, 32), :], owg.at[at(y, 32), :], y, up(d), tp)
    rsy[z] = py[at(z, ROWS), :]
    rsz[y] = pz[at(y, ROWS), :]

    seq = lax.broadcasted_iota(jnp.int32, (ROWS, 512), 0) % SEQ
    for q in range(SEQ):
        u = jnp.where(seq == q, ubuf[...], 0.0)
        grown = lax.dot_general(u, bbuf[...], TN, precision=HIGHEST, preferred_element_type=F32)
        for h in range(8):
            lo = 512 * q + 64 * h
            old = jnp.broadcast_to(kept[q : q + 1, 64 * h : 64 * h + 1], (64, 128))
            new = old * base_m[lo : lo + 64, :] + grown[64 * h : 64 * h + 64, :]
            root_m[lo : lo + 64, :] = new
            rootb[lo : lo + 64, :] = new.astype(BF16)

    outs = []

    def put(src, dst):
        c = pltpu.make_async_copy(src, dst, out_sem.at[len(outs)])
        c.start()
        outs.append(c)

    put(root_m, root_o)
    put(ns_m, ns_o)

    for d in FAR + NEAR:
        zz, yy = (z + d) % N, (y + d) % N
        arrived(RSY, zz, rsy.at[zz])
        arrived(RSZ, yy, rsz.at[yy])

    def summed(ref, lo, hi):
        total = ref[0, :, lo:hi].astype(F32)
        for s in range(1, N):
            total = total + ref[s, :, lo:hi].astype(F32)
        return total.astype(BF16).astype(F32)

    rrv[12:28, :] = summed(rsy, 0, 512)
    rrb[12:28, :] = summed(rsy, 512, 640)
    rrc[12:28, :] = summed(rsz, 512, 640)
    gate = summed(rsz, 0, 512)
    x = silu(conv(rrv, cv_m))
    b = silu(conv(rrb, cb_m))
    c = silu(conv(rrc, cc_m))
    xb[12:28, :] = x
    bb[12:28, :] = b
    c16 = c.astype(BF16)
    carried = jnp.zeros((ROWS, 512), F32)
    for q in range(SEQ):
        one = lax.dot_general(
            c16, rootb[512 * q : 512 * q + 512, :], NT, preferred_element_type=F32
        )
        carried = jnp.where(seq == q, one, carried)
    out = jnp.exp(logs) * carried + skip * x
    for j in range(PROP):
        lo = 12 - SEQ * j
        score = jnp.sum(c * bb[lo : lo + ROWS, :], axis=-1, keepdims=True)
        out = out + score * dj[j] * xb[lo : lo + ROWS, :]
    g = out * silu(gate)
    g = g * lax.rsqrt(jnp.mean(g * g, axis=-1, keepdims=True) + EPSILON)
    nrg[at(z, ROWS), :] = (g * og_m[...]).astype(BF16)
    for d in FAR + NEAR:
        send(O1, d, nrg.at[at(z, ROWS), :], nrg.at[at(z, ROWS), :], z, over(d), tp)

    for r in range(PAST):
        nv_m[r] = rrv[SEQ * r : SEQ * r + SEQ, :].astype(BF16)
        nb_m[r] = rrb[SEQ * r : SEQ * r + SEQ, :].astype(BF16)
        nc_m[r] = rrc[SEQ * r : SEQ * r + SEQ, :].astype(BF16)
    put(nv_m, nv_o)
    put(nb_m, nb_o)
    put(nc_m, nc_o)

    for d in FAR + NEAR:
        yy = (y + d) % N
        arrived(OW, yy, owg.at[at(yy, 32), :])
    for d in FAR + NEAR:
        zz = (z + d) % N
        arrived(O1, zz, nrg.at[at(zz, ROWS), :])
    po[...] = lax.dot_general(nrg[...], owg[...], NT, preferred_element_type=F32).astype(BF16)

    def back(d):
        zz = (z + d) % N
        return pltpu.make_async_remote_copy(
            src_ref=po.at[at(zz, ROWS), :], dst_ref=osum.at[tp], send_sem=send_sem.at[O2, d],
            recv_sem=recv_sem.at[O2, tp], device_id=(over(d), z), device_id_type=MESH,
        )

    for d in FAR + NEAR:
        back(d).start()

    @pl.when(z != tp)
    def _():
        back(0).start()

    @pl.when(z == tp)
    def _():
        osum[tp] = po[at(z, ROWS), :]

    for d in range(1, N):
        t = (tp + d) % N
        arrived(O2, t, osum.at[t])

    @pl.when(z != tp)
    def _():
        arrived(O2, tp, osum.at[tp])

    total = osum[0].astype(F32)
    for t in range(1, N):
        total = total + osum[t].astype(F32)
    for i in range(2):
        mf[i] = total[:, 128 * i : 128 * i + 128]
        for q in range(SEQ):
            mixed_m[q, :, 128 * i : 128 * i + 128] = mf.at[i][
                pl.ds(q, PROP, stride=SEQ), :
            ].astype(BF16)
    put(mixed_m, mixed_o)

    for c in sent:
        c.wait_send()
    for d in range(1, N):
        back(d).wait_send()

    @pl.when(z != tp)
    def _():
        back(0).wait_send()

    for c in outs:
        c.wait()


def on_device(
    tokens, input_gain, gate_weight, value_weight, write_weight, read_weight, step_weight,
    conv_value, conv_write, conv_read, step_bias, decay_log, skip_gain, output_gain,
    out_weight, base_state, past_value, past_write, past_read, past_step, accepted,
):
    vmem = pltpu.VMEM
    ops = (
        tokens, input_gain[None, :], gate_weight, value_weight, write_weight, read_weight,
        step_weight.T, conv_value, conv_write, conv_read, step_bias[None, :],
        decay_log[None, :], skip_gain[None, :], output_gain[None, :], out_weight.T,
        base_state.reshape(2048, 128), past_value.transpose(1, 0, 2),
        past_write.transpose(1, 0, 2), past_read.transpose(1, 0, 2), past_step, accepted,
    )
    out_shapes = [
        ((SEQ, PROP, 256), BF16), ((2048, 128), F32), ((PAST, SEQ, 512), BF16),
        ((PAST, SEQ, 128), BF16), ((PAST, SEQ, 128), BF16), ((SEQ, PROP, 8), BF16),
    ]
    scratch = [
        vmem((1, 2048), F32), vmem((64, 2048), BF16), vmem((4, 512), F32), vmem((4, 128), F32),
        vmem((4, 128), F32), vmem((1, 8), F32), vmem((1, 8), F32), vmem((1, 8), F32),
        vmem((1, 512), F32), vmem((2048, 128), F32), vmem((PAST, SEQ, 512), BF16),
        vmem((PAST, SEQ, 128), BF16), vmem((PAST, SEQ, 128), BF16), vmem((SEQ, PROP, 8), BF16),
        vmem((N, SEQ, PROP, 256), BF16), vmem((N, ROWS, 256), BF16), vmem((N, ROWS, 256), BF16),
        vmem((128, 256), BF16), vmem((128, 256), BF16), vmem((256, 640), BF16),
        vmem((256, 640), BF16), vmem((128, 640), BF16), vmem((128, 640), BF16),
        vmem((N, ROWS, 640), BF16), vmem((N, ROWS, 640), BF16), vmem((256, 512), BF16),
        vmem((128, 512), BF16), vmem((128, 256), BF16), vmem((N, ROWS, 256), BF16),
        vmem((ROWS, 2048), F32), vmem((28, 512), F32), vmem((28, 128), F32), vmem((28, 128), F32),
        vmem((28, 512), F32), vmem((28, 128), F32), vmem((28, 128), F32), vmem((ROWS, 512), F32),
        vmem((ROWS, 512), F32), vmem((ROWS, 512), F32), vmem((ROWS, 128), F32),
        vmem((28, 512), F32), vmem((28, 128), F32), vmem((28, 512), F32), vmem((28, 512), F32),
        vmem((PROP, ROWS, 512), F32), vmem((2048, 128), BF16), vmem((2, ROWS, 128), F32),
        vmem((ROWS, 128), F32),
        *(vmem(shape, dtype) for shape, dtype in out_shapes),
        pltpu.SemaphoreType.DMA((20,)),
        pltpu.SemaphoreType.DMA((6,)),
        pltpu.SemaphoreType.DMA((10, N)),
        pltpu.SemaphoreType.DMA((10, N)),
    ]
    mixed, root, nv, nb, nc, ns = pl.pallas_call(
        body,
        out_shape=[jax.ShapeDtypeStruct(shape, dtype) for shape, dtype in out_shapes],
        in_specs=[pl.BlockSpec(memory_space=pl.ANY)] * 20
        + [pl.BlockSpec(memory_space=pltpu.SMEM)],
        out_specs=[pl.BlockSpec(memory_space=pl.ANY)] * 6,
        scratch_shapes=scratch,
        compiler_params=pltpu.CompilerParams(collective_id=0, has_side_effects=True),
        name="mixer",
    )(*ops)
    return (
        mixed, root.reshape(base_state.shape), nv.transpose(1, 0, 2), nb.transpose(1, 0, 2),
        nc.transpose(1, 0, 2), ns,
    )


def solution(mesh):
    return jax.shard_map(
        on_device,
        mesh=mesh,
        in_specs=(
            P("kv", None, "tp"), P(), P("kv", "tp"), P("kv", "tp"), P("kv", "tp"), P("kv", "tp"),
            P(), P(None, "tp"), P(None, "tp"), P(None, "tp"), P("tp"), P("tp"), P("tp"), P("tp"),
            P("tp", "kv"), P("kv", "tp", None, None), P("kv", None, "tp"), P("kv", None, "tp"),
            P("kv", None, "tp"), P("kv", None, "tp"), P("kv"),
        ),
        out_specs=(
            P("kv", None, "tp"), P("kv", "tp", None, None), P("kv", None, "tp"),
            P("kv", None, "tp"), P("kv", None, "tp"), P("kv", None, "tp"),
        ),
        check_vma=False,
    )
```

time: 208 us -> 54.2 us (0.26)
  waiting for transfers between devices: 132 us -> 0 us
  Pallas kernels: 0 us -> 46.9 us
  blocking collectives: 32 us -> 0 us
  between operations: 14.3 us -> 0.66 us
  matrix products: 13.2 us -> 0 us
  other arithmetic: 8.01 us -> 0 us
    all_gather x2 -> x0, waiting for transfers between devices: 131 us -> none  [the longest x1 70.7 us: on_device(): lax.all_gather(out_weight, 'kv', axis=1, tiled=True)]
    pallas_call x0 -> x1, Pallas kernels: none -> 46.9 us  [on_device(): pl.pallas_call(body, out_shape=[jax.ShapeDtypeStruct(shape, dtype) for sh...]
    all_gather x1 -> x0, blocking collectives: 18.1 us -> none  [on_device(): whole = lax.all_gather(tokens, 'tp', axis=2, tiled=True)]
    all_to_all x1 -> x0, blocking collectives: 13.9 us -> none  [summed_on_arrival(): lax.all_to_all(pieces, axis, split_axis=0, concat_axis=0, tiled=True)]
    dot_general x10 -> x0, matrix products: 13.2 us -> none  [the longest x4 6.38 us: on_device(): jnp.dot(flat, piece, preferred_element_type=jnp.float32)]
    unnamed x21 -> x16, local copies, waits for them, and re-layouts: 0.09 us -> 6.28 us
    gather x3 -> x0, local copies, waits for them, and re-layouts: 3.99 us -> none  [the longest x1 1.39 us: advance(): lax.dynamic_slice_in_dim(past_x, taken, CONV_W - 1, 0)]
    convert_element_type x6 -> x0, other arithmetic: 2.27 us -> none  [the longest x1 0.8 us: on_device(): normed = (rows * lax.rsqrt(jnp.mean(rows * rows, axis=-1, keepdims=True)...]
  transfers between devices with their start and end apart: 2 -> 0, of which waited for: 2 -> 0; matrix products, arithmetic and copies ran while one was open for 12% -> 0% of each run, Pallas kernels for 0% -> 0%
where the time goes in v1:
time: 54.2 us; the launch traced here: 53.8 us
  Pallas kernels  46.9 us (87%)
  local copies, waits for them, and re-layouts  6.28 us (12%)
  between operations  0.66 us (1%)
    pallas_call x1, Pallas kernels, on_device(): pl.pallas_call(body, out_shape=[jax.ShapeDtypeStruct(shape, dtype) for sh...  46.9 us
    unnamed x16, local copies, waits for them, and re-layouts  6.28 us

profile of v1, /device:TPU:1, one launch (start us, length us, event | category | flops | bytes accessed | tf_op | source)
XLA Modules:
  0.0 53.8 jit_solution(4553885530452487414)
XLA Ops:
  0.6 46.9 %mixer.1 = (bf16[4,4,256]{2,1,0:T(4,128)(2,1)}, f32[2048,128]{1,0:T(8,128)}, bf16[7,4,512]{2,1,0:T(4,128)(2,1)}, bf16[7,4,128]{2,1,0:T(4,128)(2,1)}, bf16[7,4,12...) custom-call(bf16[4,4,256]{2,1,0:T(4,128)(2,1)} %tokens.1, f32[1,2048]{1,0:T(1,128)} %bitcast.21, bf16[32,512]{1,0:T(8,128)(2,1)} %gate_w.1, ...), custom_call_target="tpu_custom_call" | custom-call | tf_op jit(solution)/shard_map/mixer/pallas_call | solution.py:448
  47.5 0.0 copy-start.1
  47.5 0.7 %copy-done.1 = bf16[4,4,256]{2,1,0:T(4,128)(2,1)S(1)} copy-done((bf16[4,4,256]{2,1,0:T(4,128)(2,1)S(1)}, bf16[4,4,256]{2,1,0:T(4,128)(2,1)}, u32[]{:S(2)}) %copy-start.1) | copy-done | bytes 8216
  48.2 0.6 %copy.33 = bf16[4,4,256]{2,1,0:T(4,128)(2,1)} copy(bf16[4,4,256]{2,1,0:T(4,128)(2,1)S(1)} %copy-done.1) | data formatting | bytes 16384
  48.8 0.0 copy-start
  48.8 2.3 %copy.34 = f32[4,8,64,128]{3,2,1,0:T(8,128)} copy(f32[4,8,64,128]{3,2,1,0:T(8,128)} %bitcast.16) | data formatting | bytes 2097152
  51.2 0.0 copy-done
  51.2 0.0 copy-start.3
  51.2 0.6 %copy.35 = bf16[4,7,512]{2,0,1:T(4,128)(2,1)} copy(bf16[4,7,512]{2,0,1:T(4,128)(2,1)S(1)} %bitcast.19) | data formatting | bytes 57344
  51.8 0.1 copy-done.3
  51.9 0.0 copy-start.2
  51.9 0.6 %copy.36 = bf16[4,7,128]{2,0,1:T(4,128)(2,1)} copy(bf16[4,7,128]{2,0,1:T(4,128)(2,1)S(1)} %bitcast.23) | data formatting | bytes 14336
  52.5 0.1 copy-done.2
  52.6 0.0 copy-start.4
  52.6 0.6 %copy.37 = bf16[4,7,128]{2,0,1:T(4,128)(2,1)} copy(bf16[4,7,128]{2,0,1:T(4,128)(2,1)S(1)} %bitcast.22) | data formatting | bytes 14336
  53.2 0.1 copy-done.4
  53.2 0.6 %copy.38 = bf16[4,4,8]{2,1,0:T(4,128)(2,1)} copy(bf16[4,4,8]{2,1,0:T(4,128)(2,1)S(1)} %copy-done.4) | data formatting | bytes 512
Async XLA Ops:
  47.5 0.7 %copy-start.1 = (bf16[4,4,256]{2,1,0:T(4,128)(2,1)S(1)}, bf16[4,4,256]{2,1,0:T(4,128)(2,1)}, u32[]{:S(2)}) copy-start(bf16[4,4,256]{2,1,0:T(4,128)(2,1)} %get-tuple-element.24) | copy-start | bytes 24580
  48.8 2.3 %copy-start = (bf16[7,4,512]{2,1,0:T(4,128)(2,1)S(1)}, bf16[7,4,512]{2,1,0:T(4,128)(2,1)}, u32[]{:S(2)}) copy-start(bf16[7,4,512]{2,1,0:T(4,128)(2,1)} %get-tuple-element.14) | copy-start | bytes 86020
  51.2 0.7 %copy-start.3 = (bf16[7,4,128]{2,1,0:T(4,128)(2,1)S(1)}, bf16[7,4,128]{2,1,0:T(4,128)(2,1)}, u32[]{:S(2)}) copy-start(bf16[7,4,128]{2,1,0:T(4,128)(2,1)} %get-tuple-element.15) | copy-start | bytes 21508
  51.9 0.7 %copy-start.2 = (bf16[7,4,128]{2,1,0:T(4,128)(2,1)S(1)}, bf16[7,4,128]{2,1,0:T(4,128)(2,1)}, u32[]{:S(2)}) copy-start(bf16[7,4,128]{2,1,0:T(4,128)(2,1)} %get-tuple-element.16) | copy-start | bytes 21508
  52.6 0.7 %copy-start.4 = (bf16[4,4,8]{2,1,0:T(4,128)(2,1)S(1)}, bf16[4,4,8]{2,1,0:T(4,128)(2,1)}, u32[]{:S(2)}) copy-start(bf16[4,4,8]{2,1,0:T(4,128)(2,1)} %get-tuple-element.29) | copy-start | bytes 772

commit v2 on v1

--- a/solution.py
+++ b/solution.py
@@ -44,13 +44,13 @@
     tokens, input_gain, gate_w, value_w, write_w, read_w, step_w,
     conv_v, conv_b, conv_c, step_bias, decay_log, skip_gain, output_gain,
     out_w, base, past_v, past_b, past_c, past_s, accepted,
-    mixed_o, root_o, nv_o, nb_o, nc_o, ns_o,
+    mixed_m, root_m, nv_m, nb_m, nc_m, ns_m,
     gain_m, stepw_m, cv_m, cb_m, cc_m, bias_m, decay_m, skip_m, og_m,
     base_m, pv_m, pb_m, pc_m, ps_m,
     xall, nrm, npk, ay, az, wy, wz, py, pz, rsy, rsz, owg, nrg, po, osum,
     xf, ppv, ppb, ppc, rrv, rrb, rrc, stp, sbuf, ubuf, bbuf, xb, bb, lb, dtb, dj, rootb, mf, nsf,
-    mixed_m, root_m, nv_m, nb_m, nc_m, ns_m,
-    in_sem, out_sem, send_sem, recv_sem,
+    taken_m,
+    in_sem, send_sem, recv_sem,
 ):
     kv = lax.axis_index("kv")
     tp = lax.axis_index("tp")
@@ -81,6 +81,7 @@
         (output_gain, og_m),
         (step_w, stepw_m),
         (base, base_m),
+        (accepted, taken_m),
     ]
     loads = [pltpu.make_async_copy(s, d, in_sem.at[i]) for i, (s, d) in enumerate(ins)]
     for c in loads:
@@ -230,9 +231,9 @@
 
     def taken(shape):
         seq = lax.broadcasted_iota(jnp.int32, shape, 0) % SEQ
-        count = jnp.full(shape, accepted[0], jnp.int32)
+        count = jnp.full(shape, taken_m[0], jnp.int32)
         for q in range(1, SEQ):
-            count = jnp.where(seq == q, accepted[q], count)
+            count = jnp.where(seq == q, taken_m[q], count)
         return count
 
     live = lax.broadcasted_iota(jnp.int32, (ROWS, 512), 0) // SEQ < taken((ROWS, 512))
@@ -291,16 +292,6 @@
             new = old * base_m[lo : lo + 64, :] + grown[64 * h : 64 * h + 64, :]
             root_m[lo : lo + 64, :] = new
             rootb[lo : lo + 64, :] = new.astype(BF16)
-
-    outs = []
-
-    def put(src, dst):
-        c = pltpu.make_async_copy(src, dst, out_sem.at[len(outs)])
-        c.start()
-        outs.append(c)
-
-    put(root_m, root_o)
-    put(ns_m, ns_o)
 
     for d in FAR + NEAR:
         zz, yy = (z + d) % N, (y + d) % N
@@ -344,9 +335,6 @@
         nv_m[r] = rrv[SEQ * r : SEQ * r + SEQ, :].astype(BF16)
         nb_m[r] = rrb[SEQ * r : SEQ * r + SEQ, :].astype(BF16)
         nc_m[r] = rrc[SEQ * r : SEQ * r + SEQ, :].astype(BF16)
-    put(nv_m, nv_o)
-    put(nb_m, nb_o)
-    put(nc_m, nc_o)
 
     for d in FAR + NEAR:
         yy = (y + d) % N
@@ -391,7 +379,6 @@
             mixed_m[q, :, 128 * i : 128 * i + 128] = mf.at[i][
                 pl.ds(q, PROP, stride=SEQ), :
             ].astype(BF16)
-    put(mixed_m, mixed_o)
 
     for c in sent:
         c.wait_send()
@@ -402,7 +389,13 @@
     def _():
         back(0).wait_send()
 
-    for c in outs:
+
+def finish(*refs):
+    ins, outs, sem = refs[:6], refs[6:12], refs[12]
+    copies = [pltpu.make_async_copy(s, d, sem.at[i]) for i, (s, d) in enumerate(zip(ins, outs))]
+    for c in copies:
+        c.start()
+    for c in copies:
         c.wait()
 
 
@@ -439,22 +432,28 @@
         vmem((28, 512), F32), vmem((28, 128), F32), vmem((28, 512), F32), vmem((28, 512), F32),
         vmem((PROP, ROWS, 512), F32), vmem((2048, 128), BF16), vmem((2, ROWS, 128), F32),
         vmem((ROWS, 128), F32),
-        *(vmem(shape, dtype) for shape, dtype in out_shapes),
-        pltpu.SemaphoreType.DMA((20,)),
-        pltpu.SemaphoreType.DMA((6,)),
+        pltpu.SMEM((SEQ,), jnp.int32),
+        pltpu.SemaphoreType.DMA((21,)),
         pltpu.SemaphoreType.DMA((10, N)),
         pltpu.SemaphoreType.DMA((10, N)),
     ]
-    mixed, root, nv, nb, nc, ns = pl.pallas_call(
+    held = pl.pallas_call(
         body,
-        out_shape=[jax.ShapeDtypeStruct(shape, dtype) for shape, dtype in out_shapes],
-        in_specs=[pl.BlockSpec(memory_space=pl.ANY)] * 20
-        + [pl.BlockSpec(memory_space=pltpu.SMEM)],
-        out_specs=[pl.BlockSpec(memory_space=pl.ANY)] * 6,
+        out_shape=[vmem(shape, dtype) for shape, dtype in out_shapes],
+        in_specs=[pl.BlockSpec(memory_space=pl.ANY)] * 21,
+        out_specs=[pl.BlockSpec(memory_space=vmem)] * 6,
         scratch_shapes=scratch,
         compiler_params=pltpu.CompilerParams(collective_id=0, has_side_effects=True),
         name="mixer",
     )(*ops)
+    mixed, root, nv, nb, nc, ns = pl.pallas_call(
+        finish,
+        out_shape=[jax.ShapeDtypeStruct(shape, dtype) for shape, dtype in out_shapes],
+        in_specs=[pl.BlockSpec(memory_space=vmem)] * 6,
+        out_specs=[pl.BlockSpec(memory_space=pl.ANY)] * 6,
+        scratch_shapes=[pltpu.SemaphoreType.DMA((6,))],
+        name="finish",
+    )(*(pltpu.with_memory_space_constraint(h, vmem) for h in held))
     return (
         mixed, root.reshape(base_state.shape), nv.transpose(1, 0, 2), nb.transpose(1, 0, 2),
         nc.transpose(1, 0, 2), ns,

time: 54.2 us -> 47.5 us (0.88)
  local copies, waits for them, and re-layouts: 6.28 us -> 0 us
    unnamed x16 -> x0, local copies, waits for them, and re-layouts: 6.28 us -> none
    pallas_call x1 -> x2, Pallas kernels: 46.9 us -> 46.7 us  [the longest x1 45.7 us: on_device(): pl.pallas_call(body, out_shape=[vmem(shape, dtype) for shape, dtype in ou...]
where the time goes in v2:
time: 47.5 us; the launch traced here: 47.4 us
  Pallas kernels  46.7 us (98%)
  between operations  0.65 us (1%)
    pallas_call x1, Pallas kernels, on_device(): pl.pallas_call(body, out_shape=[vmem(shape, dtype) for shape, dtype in ou...  45.7 us
    pallas_call x1, Pallas kernels, on_device(): pl.pallas_call(finish, out_shape=[jax.ShapeDtypeStruct(shape, dtype) for...  1.04 us

profile of v2, /device:TPU:1, one launch (start us, length us, event | category | flops | bytes accessed | tf_op | source)
XLA Modules:
  0.0 47.4 jit_solution(13857115399964017872)
XLA Ops:
  0.6 45.7 %mixer.1 = (bf16[4,4,256]{2,1,0:T(4,128)(2,1)S(1)}, f32[2048,128]{1,0:T(8,128)S(1)}, bf16[7,4,512]{2,1,0:T(4,128)(2,1)S(1)}, bf16[7,4,128]{2,1,0:T(4,128)(2,1)S(...) custom-call(bf16[4,4,256]{2,1,0:T(4,128)(2,1)} %tokens.1, f32[1,2048]{1,0:T(1,128)} %bitcast.19, ...), custom_call_target="tpu_custom_call" | custom-call | tf_op jit(solution)/shard_map/mixer/pallas_call | solution.py:440
  46.4 1.0 %finish.1 = (bf16[4,4,256]{2,1,0:T(4,128)(2,1)}, f32[2048,128]{1,0:T(8,128)}, bf16[7,4,512]{2,1,0:T(4,128)(2,1)}, bf16[7,4,128]{2,1,0:T(4,128)(2,1)}, bf16[7,4,1...) custom-call(bf16[4,4,256]{2,1,0:T(4,128)(2,1)S(1)} %get-tuple-element.18.refs_0_, f32[2048,128]{1,0:T(8,128)S(1)} %get-tuple-element.19.refs_1_, ...), custom_call_target="tpu_custom_call" | custom-call | tf_op jit(solution)/shard_map/finish/pallas_call | solution.py:449

commit v3 on v2

--- a/solution.py
+++ b/solution.py
@@ -19,8 +19,7 @@
 PAST = 7
 NT = (((1,), (1,)), ((), ()))
 TN = (((0,), (0,)), ((), ()))
-FAR = (4, 3, 5)
-NEAR = (2, 6, 1, 7)
+ORDER = (4, 3, 5, 2, 6, 1, 7)
 
 T1, T2Y, T2Z, WY, WZ, RSY, RSZ, OW, O1, O2 = range(10)
 
@@ -96,15 +95,10 @@
         tell(kv, (tp + d) % N)
         tell(z * N + (y + d) % N, tp)
         tell(((z + d) % N) * N + y, tp)
-        tell(tp * N + y, (tp + d) % N)
-
-    @pl.when(z != tp)
-    def _():
-        tell(tp * N + y, tp)
 
     for c in loads[:6]:
         c.wait()
-    pl.semaphore_wait(barrier, 4 * (N - 1) + jnp.where(z != tp, 1, 0).astype(jnp.int32))
+    pl.semaphore_wait(barrier, 3 * (N - 1))
 
     sent = []
 
@@ -128,14 +122,32 @@
     def over(d):
         return ((z + d) % N) * N + y
 
-    def weights(ds):
-        for d in ds:
-            send(WY, d, wy.at[at(y, 32), :], wy.at[at(y, 32), :], y, up(d), tp)
-            send(WZ, d, wz.at[at(z, 32), :], wz.at[at(z, 32), :], z, over(d), tp)
+    def slab(owner, h):
+        return pl.ds(pl.multiple_of(owner * 32 + 16 * h, 16), 16)
+
+    def spread_own(phase, ref, me, dev):
+        for d in (2, 6, 1, 7):
+            send(phase, d, ref.at[at(me, 32), :], ref.at[at(me, 32), :], me, dev(d), tp)
+
+    def spread_on(phase, ref, me, dev):
+        for h, back_two, on in ((0, 6, (1, 2)), (1, 2, (7, 6))):
+            owner = (me + back_two) % N
+            block, part = ref.at[at(owner, 32), :], ref.at[slab(owner, h), :]
+            arrived(phase, owner, block)
+            send(phase, 3 + 2 * h, block, block, owner, dev(on[0]), tp)
+            send(phase, 4 - 4 * h, part, part, N + h, dev(on[1]), tp)
+
+    def spread_end(phase, ref, me):
+        for d in (1, 7, 3, 5):
+            owner = (me + d) % N
+            arrived(phase, owner, ref.at[at(owner, 32), :])
+        for h in range(2):
+            arrived(phase, N + h, ref.at[slab((me + 4) % N, h), :])
 
     for d in range(1, N):
         send(T1, d, xall.at[tp], xall.at[tp], tp, kv, (tp + d) % N)
-    weights(FAR)
+    spread_own(WY, wy, y, up)
+    spread_own(WZ, wz, z, over)
 
     for c in loads[6:]:
         c.wait()
@@ -174,11 +186,12 @@
             npk[yy, :, 128 * half : 128 * half + 128] = tile.astype(BF16)
     ay[at(z, ROWS), :] = nrm[z]
     az[at(y, ROWS), :] = npk[y]
-    for d in FAR + NEAR:
+    for d in ORDER:
         zz, yy = (z + d) % N, (y + d) % N
         send(T2Y, d, nrm.at[zz], ay.at[at(z, ROWS), :], z, over(d), tp)
         send(T2Z, d, npk.at[yy], az.at[at(y, ROWS), :], y, up(d), tp)
-    weights(NEAR)
+    spread_on(WY, wy, y, up)
+    spread_on(WZ, wz, z, over)
 
     head = lax.broadcasted_iota(jnp.int32, (1, 512), 1) // 64
 
@@ -265,20 +278,15 @@
         zz, yy = (z + d) % N, (y + d) % N
         arrived(T2Y, zz, ay.at[at(zz, ROWS), :])
         arrived(T2Z, yy, az.at[at(yy, ROWS), :])
-    for d in FAR + NEAR:
-        yy = (y + d) % N
-        arrived(WY, yy, wy.at[at(yy, 32), :])
+    spread_end(WY, wy, y)
     py[...] = jnp.dot(ay[...], wy[...], preferred_element_type=F32).astype(BF16)
-    for d in FAR + NEAR:
-        zz = (z + d) % N
-        arrived(WZ, zz, wz.at[at(zz, 32), :])
+    spread_end(WZ, wz, z)
     pz[...] = jnp.dot(az[...], wz[...], preferred_element_type=F32).astype(BF16)
-    for d in FAR + NEAR:
+    for d in ORDER:
         zz, yy = (z + d) % N, (y + d) % N
         send(RSY, d, py.at[at(zz, ROWS), :], rsy.at[z], z, over(d), tp)
         send(RSZ, d, pz.at[at(yy, ROWS), :], rsz.at[y], y, up(d), tp)
-    for d in FAR + NEAR:
-        send(OW, d, owg.at[at(y, 32), :], owg.at[at(y, 32), :], y, up(d), tp)
+    spread_own(OW, owg, y, up)
     rsy[z] = py[at(z, ROWS), :]
     rsz[y] = pz[at(y, ROWS), :]
 
@@ -293,7 +301,7 @@
             root_m[lo : lo + 64, :] = new
             rootb[lo : lo + 64, :] = new.astype(BF16)
 
-    for d in FAR + NEAR:
+    for d in ORDER:
         zz, yy = (z + d) % N, (y + d) % N
         arrived(RSY, zz, rsy.at[zz])
         arrived(RSZ, yy, rsz.at[yy])
@@ -328,18 +336,17 @@
     g = out * silu(gate)
     g = g * lax.rsqrt(jnp.mean(g * g, axis=-1, keepdims=True) + EPSILON)
     nrg[at(z, ROWS), :] = (g * og_m[...]).astype(BF16)
-    for d in FAR + NEAR:
+    for d in ORDER:
         send(O1, d, nrg.at[at(z, ROWS), :], nrg.at[at(z, ROWS), :], z, over(d), tp)
+    spread_on(OW, owg, y, up)
 
     for r in range(PAST):
         nv_m[r] = rrv[SEQ * r : SEQ * r + SEQ, :].astype(BF16)
         nb_m[r] = rrb[SEQ * r : SEQ * r + SEQ, :].astype(BF16)
         nc_m[r] = rrc[SEQ * r : SEQ * r + SEQ, :].astype(BF16)
 
-    for d in FAR + NEAR:
-        yy = (y + d) % N
-        arrived(OW, yy, owg.at[at(yy, 32), :])
-    for d in FAR + NEAR:
+    spread_end(OW, owg, y)
+    for d in ORDER:
         zz = (z + d) % N
         arrived(O1, zz, nrg.at[at(zz, ROWS), :])
     po[...] = lax.dot_general(nrg[...], owg[...], NT, preferred_element_type=F32).astype(BF16)
@@ -351,7 +358,7 @@
             recv_sem=recv_sem.at[O2, tp], device_id=(over(d), z), device_id_type=MESH,
         )
 
-    for d in FAR + NEAR:
+    for d in ORDER:
         back(d).start()
 
     @pl.when(z != tp)
@@ -435,7 +442,7 @@
         pltpu.SMEM((SEQ,), jnp.int32),
         pltpu.SemaphoreType.DMA((21,)),
         pltpu.SemaphoreType.DMA((10, N)),
-        pltpu.SemaphoreType.DMA((10, N)),
+        pltpu.SemaphoreType.DMA((10, N + 2)),
     ]
     held = pl.pallas_call(
         body,

time: 47.5 us -> 45.6 us (0.960)
  Pallas kernels: 46.7 us -> 44.8 us
    pallas_call x1, Pallas kernels: 45.7 us -> 43.8 us  [on_device(): pl.pallas_call(body, out_shape=[vmem(shape, dtype) for shape, dtype in ou...]
where the time goes in v3:
time: 45.6 us; the launch traced here: 45.5 us
  Pallas kernels  44.8 us (98%)
  between operations  0.65 us (1%)
    pallas_call x1, Pallas kernels, on_device(): pl.pallas_call(body, out_shape=[vmem(shape, dtype) for shape, dtype in ou...  43.8 us
    pallas_call x1, Pallas kernels, on_device(): pl.pallas_call(finish, out_shape=[jax.ShapeDtypeStruct(shape, dtype) for...  1.04 us

profile of v3, /device:TPU:1, one launch (start us, length us, event | category | flops | bytes accessed | tf_op | source)
XLA Modules:
  0.0 45.5 jit_solution(4118831989232189779)
XLA Ops:
  0.6 43.8 %mixer.1 = (bf16[4,4,256]{2,1,0:T(4,128)(2,1)S(1)}, f32[2048,128]{1,0:T(8,128)S(1)}, bf16[7,4,512]{2,1,0:T(4,128)(2,1)S(1)}, bf16[7,4,128]{2,1,0:T(4,128)(2,1)S(...) custom-call(bf16[4,4,256]{2,1,0:T(4,128)(2,1)} %tokens.1, f32[1,2048]{1,0:T(1,128)} %bitcast.19, ...), custom_call_target="tpu_custom_call" | custom-call | tf_op jit(solution)/shard_map/mixer/pallas_call | solution.py:447
  44.4 1.0 %finish.1 = (bf16[4,4,256]{2,1,0:T(4,128)(2,1)}, f32[2048,128]{1,0:T(8,128)}, bf16[7,4,512]{2,1,0:T(4,128)(2,1)}, bf16[7,4,128]{2,1,0:T(4,128)(2,1)}, bf16[7,4,1...) custom-call(bf16[4,4,256]{2,1,0:T(4,128)(2,1)S(1)} %get-tuple-element.18.refs_0_, f32[2048,128]{1,0:T(8,128)S(1)} %get-tuple-element.19.refs_1_, ...), custom_call_target="tpu_custom_call" | custom-call | tf_op jit(solution)/shard_map/finish/pallas_call | solution.py:456

commit v4 on v3

--- a/solution.py
+++ b/solution.py
@@ -45,11 +45,11 @@
     out_w, base, past_v, past_b, past_c, past_s, accepted,
     mixed_m, root_m, nv_m, nb_m, nc_m, ns_m,
     gain_m, stepw_m, cv_m, cb_m, cc_m, bias_m, decay_m, skip_m, og_m,
-    base_m, pv_m, pb_m, pc_m, ps_m,
+    base_m, pv_m, pb_m, pc_m, ps_m, tok_m,
     xall, nrm, npk, ay, az, wy, wz, py, pz, rsy, rsz, owg, nrg, po, osum,
     xf, ppv, ppb, ppc, rrv, rrb, rrc, stp, sbuf, ubuf, bbuf, xb, bb, lb, dtb, dj, rootb, mf, nsf,
     taken_m,
-    in_sem, send_sem, recv_sem,
+    in_sem, send_sem, recv_sem, hello,
 ):
     kv = lax.axis_index("kv")
     tp = lax.axis_index("tp")
@@ -59,32 +59,48 @@
     def at(rows, count):
         return pl.ds(pl.multiple_of(rows * count, count), count)
 
-    ins = [
-        (value_w, wy.at[at(y, 32), pl.ds(0, 512)]),
-        (write_w, wy.at[at(y, 32), pl.ds(512, 128)]),
-        (gate_w, wz.at[at(z, 32), pl.ds(0, 512)]),
-        (read_w, wz.at[at(z, 32), pl.ds(512, 128)]),
-        (out_w, owg.at[at(y, 32), :]),
-        (tokens, xall.at[tp]),
-        (input_gain, gain_m),
-        (past_v, pv_m),
-        (past_b, pb_m),
-        (past_c, pc_m),
-        (past_s, ps_m),
-        (conv_v, cv_m),
-        (conv_b, cb_m),
-        (conv_c, cc_m),
-        (step_bias, bias_m),
-        (decay_log, decay_m),
-        (skip_gain, skip_m),
-        (output_gain, og_m),
-        (step_w, stepw_m),
-        (base, base_m),
-        (accepted, taken_m),
-    ]
-    loads = [pltpu.make_async_copy(s, d, in_sem.at[i]) for i, (s, d) in enumerate(ins)]
-    for c in loads:
-        c.start()
+    def up(d):
+        return z * N + (y + d) % N
+
+    def over(d):
+        return ((z + d) % N) * N + y
+
+    groups = (
+        (
+            (value_w, wy.at[at(y, 32), pl.ds(0, 512)]),
+            (write_w, wy.at[at(y, 32), pl.ds(512, 128)]),
+            (gate_w, wz.at[at(z, 32), pl.ds(0, 512)]),
+            (read_w, wz.at[at(z, 32), pl.ds(512, 128)]),
+            (out_w, owg.at[at(y, 32), :]),
+            (tokens, tok_m),
+        ),
+        (
+            (input_gain, gain_m),
+            (past_v, pv_m),
+            (past_b, pb_m),
+            (past_c, pc_m),
+            (conv_v, cv_m),
+            (conv_b, cb_m),
+            (conv_c, cc_m),
+            (output_gain, og_m),
+        ),
+        ((past_s, ps_m),),
+        ((step_bias, bias_m),),
+        ((decay_log, decay_m),),
+        ((skip_gain, skip_m),),
+        ((accepted, taken_m),),
+        ((step_w, stepw_m),),
+        ((base, base_m),),
+    )
+    for i, group in enumerate(groups):
+        for source, target in group:
+            pltpu.make_async_copy(source, target, in_sem.at[i]).start()
+
+    def loaded(i, ref=None):
+        if ref is None:
+            pltpu.make_async_copy(*groups[i][0], in_sem.at[i]).wait()
+        else:
+            pltpu.make_async_copy(ref, ref, in_sem.at[i]).wait()
 
     barrier = pltpu.get_barrier_semaphore()
 
@@ -93,105 +109,117 @@
 
     for d in range(1, N):
         tell(kv, (tp + d) % N)
-        tell(z * N + (y + d) % N, tp)
-        tell(((z + d) % N) * N + y, tp)
-
-    for c in loads[:6]:
-        c.wait()
-    pl.semaphore_wait(barrier, 3 * (N - 1))
-
-    sent = []
-
-    def send(phase, d, src, dst, slot, k, t):
-        c = pltpu.make_async_remote_copy(
-            src_ref=src, dst_ref=dst, send_sem=send_sem.at[phase, d],
-            recv_sem=recv_sem.at[phase, slot], device_id=(k, t), device_id_type=MESH,
+    for d in (1, 7, 2, 6):
+        tell(up(d), tp)
+        tell(over(d), tp)
+
+    loaded(0, wy.at[pl.ds(0, 96), :])
+    to = lax.broadcasted_iota(jnp.int32, (ROWS, ROWS), 0)
+    by = lax.broadcasted_iota(jnp.int32, (ROWS, ROWS), 1)
+    swap = jnp.where((to % SEQ) * PROP + to // SEQ == by, 1.0, 0.0).astype(BF16)
+    for q in range(SEQ):
+        xf[PROP * q : PROP * q + PROP, :] = tok_m[q].astype(F32)
+    xall[tp] = jnp.dot(swap, xf[...].astype(BF16), preferred_element_type=F32).astype(BF16)
+    pl.semaphore_wait(barrier, N - 1 + 8)
+    for d in (2, 6):
+        pl.semaphore_signal(hello, inc=1, device_id=(up(d), tp), device_id_type=MESH)
+        pl.semaphore_signal(hello, inc=1, device_id=(over(d), tp), device_id_type=MESH)
+
+    def copy(phase, slot, src, dst, k, t):
+        return pltpu.make_async_remote_copy(
+            src_ref=src, dst_ref=dst, send_sem=send_sem.at[phase], recv_sem=recv_sem.at[slot],
+            device_id=(k, t), device_id_type=MESH,
         )
-        c.start()
-        sent.append(c)
-
-    def arrived(phase, slot, ref):
-        pltpu.make_async_remote_copy(
-            src_ref=ref, dst_ref=ref, send_sem=send_sem.at[phase, 0],
-            recv_sem=recv_sem.at[phase, slot], device_id=(kv, tp), device_id_type=MESH,
-        ).wait_recv()
-
-    def up(d):
-        return z * N + (y + d) % N
-
-    def over(d):
-        return ((z + d) % N) * N + y
-
-    def slab(owner, h):
-        return pl.ds(pl.multiple_of(owner * 32 + 16 * h, 16), 16)
-
-    def spread_own(phase, ref, me, dev):
-        for d in (2, 6, 1, 7):
-            send(phase, d, ref.at[at(me, 32), :], ref.at[at(me, 32), :], me, dev(d), tp)
-
-    def spread_on(phase, ref, me, dev):
-        for h, back_two, on in ((0, 6, (1, 2)), (1, 2, (7, 6))):
-            owner = (me + back_two) % N
-            block, part = ref.at[at(owner, 32), :], ref.at[slab(owner, h), :]
-            arrived(phase, owner, block)
-            send(phase, 3 + 2 * h, block, block, owner, dev(on[0]), tp)
-            send(phase, 4 - 4 * h, part, part, N + h, dev(on[1]), tp)
-
-    def spread_end(phase, ref, me):
-        for d in (1, 7, 3, 5):
-            owner = (me + d) % N
-            arrived(phase, owner, ref.at[at(owner, 32), :])
+
+    def send(phase, src, dst, k, t):
+        copy(phase, phase, src, dst, k, t).start()
+
+    def arrived(phase, ref):
+        copy(phase, phase, ref, ref, kv, tp).wait_recv()
+
+    def gone(phase, ref):
+        copy(phase, phase, ref, ref, kv, tp).wait_send()
+
+    def slab(ref, owner, h):
+        return ref.at[pl.ds(pl.multiple_of(owner * 32 + 16 * h, 16), 16), :]
+
+    def pass_slab(phase, slot, ref, owner, h, k):
+        copy(phase, slot, slab(ref, owner, h), slab(ref, owner, h), k, tp).start()
+
+    def early(first, h, side):
+        return first + 2 * h + side
+
+    def spread_own(rings):
+        for ds in ((2, 6), (1, 7)):
+            for h in range(2):
+                for side, d in enumerate(ds):
+                    for phase, first, ref, me, dev in rings:
+                        slot = early(first, h, side) if d in (2, 6) else phase
+                        pass_slab(phase, slot, ref, me, h, dev(d))
+
+    def spread_on(rings):
         for h in range(2):
-            arrived(phase, N + h, ref.at[slab((me + 4) % N, h), :])
+            for side, (back_two, one, two) in enumerate(((6, 1, 2), (2, 7, 6))):
+                for phase, first, ref, me, dev in rings:
+                    owner = (me + back_two) % N
+                    part = slab(ref, owner, h)
+                    copy(phase, early(first, h, side), part, part, kv, tp).wait_recv()
+                    pass_slab(phase, phase, ref, owner, h, dev(one))
+                    if h == side:
+                        pass_slab(phase, phase, ref, owner, h, dev(two))
+
+    def spread_end(ring):
+        arrived(ring[0], ring[2].at[pl.ds(0, 160), :])
+
+    ring_y = (WY, 10, wy, y, up)
+    ring_z = (WZ, 14, wz, z, over)
+    ring_o = (OW, 18, owg, y, up)
 
     for d in range(1, N):
-        send(T1, d, xall.at[tp], xall.at[tp], tp, kv, (tp + d) % N)
-    spread_own(WY, wy, y, up)
-    spread_own(WZ, wz, z, over)
-
-    for c in loads[6:]:
-        c.wait()
+        send(T1, xall.at[tp], xall.at[tp], kv, (tp + d) % N)
+    spread_own((ring_y, ring_z))
+
+    loaded(1, base_m.at[pl.ds(0, 128), :])
+    for i in range(2, 9):
+        loaded(i)
     for r in range(PAST):
         ppv[SEQ * r : SEQ * r + SEQ, :] = pv_m[r].astype(F32)
         ppb[SEQ * r : SEQ * r + SEQ, :] = pb_m[r].astype(F32)
         ppc[SEQ * r : SEQ * r + SEQ, :] = pc_m[r].astype(F32)
 
-    for d in range(1, N):
-        t = (tp + d) % N
-        arrived(T1, t, xall.at[t])
+    arrived(T1, xall.at[pl.ds(0, N - 1)])
+    blocks = [xall[t].astype(F32) for t in range(N)]
+    square = blocks[0] * blocks[0]
+    for t in range(1, N):
+        square = square + blocks[t] * blocks[t]
+    scale = lax.rsqrt(jnp.sum(square, axis=-1, keepdims=True) * (1.0 / 2048) + EPSILON)
+    normed = []
     for t in range(N):
-        for q in range(SEQ):
-            xf[PROP * q : PROP * q + PROP, 256 * t : 256 * t + 256] = xall[t, q].astype(F32)
-    rows = xf[...]
-    scale = lax.rsqrt(jnp.mean(rows * rows, axis=-1, keepdims=True) + EPSILON)
-    normed16 = (rows * scale * gain_m[...]).astype(BF16)
-    to = lax.broadcasted_iota(jnp.int32, (ROWS, ROWS), 0)
-    by = lax.broadcasted_iota(jnp.int32, (ROWS, ROWS), 1)
-    swap = jnp.where((to % SEQ) * PROP + to // SEQ == by, 1.0, 0.0).astype(BF16)
-    normed = jnp.dot(swap, normed16, preferred_element_type=F32)
-    normed16 = normed.astype(BF16)
-    for zz in range(N):
-        nrm[zz] = normed16[:, 256 * zz : 256 * zz + 256]
+        block = (blocks[t] * scale * gain_m[:, 256 * t : 256 * t + 256]).astype(BF16)
+        nrm[t] = block
+        normed.append(block.astype(F32))
+    ay[at(z, ROWS), :] = nrm[z]
+    pl.semaphore_wait(hello, 4)
+    for d in ORDER:
+        zz = (z + d) % N
+        send(T2Y, nrm.at[zz], ay.at[at(z, ROWS), :], over(d), tp)
     lane = lax.broadcasted_iota(jnp.int32, (ROWS, 128), 1) // 32
     for yy in range(N):
         for half in range(2):
             tile = None
             for i in range(4):
-                start = 256 * (4 * half + i) + 128 * (yy // 4)
                 shift = (32 * i - 32 * (yy % 4)) % 128
-                piece = normed[:, start : start + 128]
+                start = 128 * (yy // 4)
+                piece = normed[4 * half + i][:, start : start + 128]
                 if shift:
                     piece = pltpu.roll(piece, shift, 1)
                 tile = piece if tile is None else jnp.where(lane == i, piece, tile)
             npk[yy, :, 128 * half : 128 * half + 128] = tile.astype(BF16)
-    ay[at(z, ROWS), :] = nrm[z]
     az[at(y, ROWS), :] = npk[y]
     for d in ORDER:
-        zz, yy = (z + d) % N, (y + d) % N
-        send(T2Y, d, nrm.at[zz], ay.at[at(z, ROWS), :], z, over(d), tp)
-        send(T2Z, d, npk.at[yy], az.at[at(y, ROWS), :], y, up(d), tp)
-    spread_on(WY, wy, y, up)
-    spread_on(WZ, wz, z, over)
+        yy = (y + d) % N
+        send(T2Z, npk.at[yy], az.at[at(y, ROWS), :], up(d), tp)
+    spread_on((ring_y, ring_z))
 
     head = lax.broadcasted_iota(jnp.int32, (1, 512), 1) // 64
 
@@ -204,7 +232,11 @@
     bias = spread(bias_m)
     rate = jnp.exp(spread(decay_m))
     skip = spread(skip_m)
-    step16 = lax.dot_general(normed16, stepw_m[...], NT, preferred_element_type=F32).astype(BF16)
+    step = jnp.zeros((ROWS, 64), F32)
+    for t in range(N):
+        weight = stepw_m[:, 256 * t : 256 * t + 256]
+        step = step + lax.dot_general(nrm[t], weight, NT, preferred_element_type=F32)
+    step16 = step.astype(BF16)
     row64 = lax.broadcasted_iota(jnp.int32, (64, 512), 0)
     own64 = (row64 - 8 * tp == lax.broadcasted_iota(jnp.int32, (64, 512), 1) // 64)
     wide = jnp.dot(step16, jnp.where(own64, 1.0, 0.0).astype(BF16), preferred_element_type=F32)
@@ -274,19 +306,17 @@
     window(ppb, rrb, 128)
     window(ppc, rrc, 128)
 
-    for d in range(1, N):
-        zz, yy = (z + d) % N, (y + d) % N
-        arrived(T2Y, zz, ay.at[at(zz, ROWS), :])
-        arrived(T2Z, yy, az.at[at(yy, ROWS), :])
-    spread_end(WY, wy, y)
+    rest = pl.ds(0, ROWS * (N - 1))
+    arrived(T2Y, ay.at[rest, :])
+    arrived(T2Z, az.at[rest, :])
+    spread_end(ring_y)
     py[...] = jnp.dot(ay[...], wy[...], preferred_element_type=F32).astype(BF16)
-    spread_end(WZ, wz, z)
+    spread_end(ring_z)
     pz[...] = jnp.dot(az[...], wz[...], preferred_element_type=F32).astype(BF16)
     for d in ORDER:
         zz, yy = (z + d) % N, (y + d) % N
-        send(RSY, d, py.at[at(zz, ROWS), :], rsy.at[z], z, over(d), tp)
-        send(RSZ, d, pz.at[at(yy, ROWS), :], rsz.at[y], y, up(d), tp)
-    spread_own(OW, owg, y, up)
+        send(RSY, py.at[at(zz, ROWS), :], rsy.at[z], over(d), tp)
+        send(RSZ, pz.at[at(yy, ROWS), :], rsz.at[y], up(d), tp)
     rsy[z] = py[at(z, ROWS), :]
     rsz[y] = pz[at(y, ROWS), :]
 
@@ -301,10 +331,10 @@
             root_m[lo : lo + 64, :] = new
             rootb[lo : lo + 64, :] = new.astype(BF16)
 
-    for d in ORDER:
-        zz, yy = (z + d) % N, (y + d) % N
-        arrived(RSY, zz, rsy.at[zz])
-        arrived(RSZ, yy, rsz.at[yy])
+    spread_own((ring_o,))
+
+    arrived(RSY, rsy.at[pl.ds(0, N - 1)])
+    arrived(RSZ, rsz.at[pl.ds(0, N - 1)])
 
     def summed(ref, lo, hi):
         total = ref[0, :, lo:hi].astype(F32)
@@ -337,45 +367,34 @@
     g = g * lax.rsqrt(jnp.mean(g * g, axis=-1, keepdims=True) + EPSILON)
     nrg[at(z, ROWS), :] = (g * og_m[...]).astype(BF16)
     for d in ORDER:
-        send(O1, d, nrg.at[at(z, ROWS), :], nrg.at[at(z, ROWS), :], z, over(d), tp)
-    spread_on(OW, owg, y, up)
+        send(O1, nrg.at[at(z, ROWS), :], nrg.at[at(z, ROWS), :], over(d), tp)
+    spread_on((ring_o,))
 
     for r in range(PAST):
         nv_m[r] = rrv[SEQ * r : SEQ * r + SEQ, :].astype(BF16)
         nb_m[r] = rrb[SEQ * r : SEQ * r + SEQ, :].astype(BF16)
         nc_m[r] = rrc[SEQ * r : SEQ * r + SEQ, :].astype(BF16)
 
-    spread_end(OW, owg, y)
-    for d in ORDER:
-        zz = (z + d) % N
-        arrived(O1, zz, nrg.at[at(zz, ROWS), :])
+    spread_end(ring_o)
+    arrived(O1, nrg.at[rest, :])
     po[...] = lax.dot_general(nrg[...], owg[...], NT, preferred_element_type=F32).astype(BF16)
 
     def back(d):
         zz = (z + d) % N
-        return pltpu.make_async_remote_copy(
-            src_ref=po.at[at(zz, ROWS), :], dst_ref=osum.at[tp], send_sem=send_sem.at[O2, d],
-            recv_sem=recv_sem.at[O2, tp], device_id=(over(d), z), device_id_type=MESH,
-        )
+        send(O2, po.at[at(zz, ROWS), :], osum.at[tp], over(d), z)
 
     for d in ORDER:
-        back(d).start()
+        back(d)
 
     @pl.when(z != tp)
     def _():
-        back(0).start()
+        back(0)
+        arrived(O2, osum)
 
     @pl.when(z == tp)
     def _():
         osum[tp] = po[at(z, ROWS), :]
-
-    for d in range(1, N):
-        t = (tp + d) % N
-        arrived(O2, t, osum.at[t])
-
-    @pl.when(z != tp)
-    def _():
-        arrived(O2, tp, osum.at[tp])
+        arrived(O2, osum.at[pl.ds(0, N - 1)])
 
     total = osum[0].astype(F32)
     for t in range(1, N):
@@ -387,19 +406,30 @@
                 pl.ds(q, PROP, stride=SEQ), :
             ].astype(BF16)
 
-    for c in sent:
-        c.wait_send()
-    for d in range(1, N):
-        back(d).wait_send()
+    gone(T1, xall.at[pl.ds(0, N - 1)])
+    gone(T2Y, ay.at[rest, :])
+    gone(T2Z, az.at[rest, :])
+    gone(WY, wy.at[pl.ds(0, 224), :])
+    gone(WZ, wz.at[pl.ds(0, 224), :])
+    gone(RSY, rsy.at[pl.ds(0, N - 1)])
+    gone(RSZ, rsz.at[pl.ds(0, N - 1)])
+    gone(OW, owg.at[pl.ds(0, 224), :])
+    gone(O1, nrg.at[rest, :])
 
     @pl.when(z != tp)
     def _():
-        back(0).wait_send()
+        gone(O2, osum)
+
+    @pl.when(z == tp)
+    def _():
+        gone(O2, osum.at[pl.ds(0, N - 1)])
 
 
 def finish(*refs):
     ins, outs, sem = refs[:6], refs[6:12], refs[12]
-    copies = [pltpu.make_async_copy(s, d, sem.at[i]) for i, (s, d) in enumerate(zip(ins, outs))]
+    pairs = [(s, d) for i, (s, d) in enumerate(zip(ins, outs)) if i != 1]
+    pairs += [(ins[1].at[part], outs[1].at[part]) for part in (pl.ds(512 * i, 512) for i in range(4))]
+    copies = [pltpu.make_async_copy(s, d, sem.at[i]) for i, (s, d) in enumerate(pairs)]
     for c in copies:
         c.start()
     for c in copies:
@@ -428,21 +458,23 @@
         vmem((4, 128), F32), vmem((1, 8), F32), vmem((1, 8), F32), vmem((1, 8), F32),
         vmem((1, 512), F32), vmem((2048, 128), F32), vmem((PAST, SEQ, 512), BF16),
         vmem((PAST, SEQ, 128), BF16), vmem((PAST, SEQ, 128), BF16), vmem((SEQ, PROP, 8), BF16),
-        vmem((N, SEQ, PROP, 256), BF16), vmem((N, ROWS, 256), BF16), vmem((N, ROWS, 256), BF16),
+        vmem((SEQ, PROP, 256), BF16),
+        vmem((N, ROWS, 256), BF16), vmem((N, ROWS, 256), BF16), vmem((N, ROWS, 256), BF16),
         vmem((128, 256), BF16), vmem((128, 256), BF16), vmem((256, 640), BF16),
         vmem((256, 640), BF16), vmem((128, 640), BF16), vmem((128, 640), BF16),
         vmem((N, ROWS, 640), BF16), vmem((N, ROWS, 640), BF16), vmem((256, 512), BF16),
         vmem((128, 512), BF16), vmem((128, 256), BF16), vmem((N, ROWS, 256), BF16),
-        vmem((ROWS, 2048), F32), vmem((28, 512), F32), vmem((28, 128), F32), vmem((28, 128), F32),
+        vmem((ROWS, 256), F32), vmem((28, 512), F32), vmem((28, 128), F32), vmem((28, 128), F32),
         vmem((28, 512), F32), vmem((28, 128), F32), vmem((28, 128), F32), vmem((ROWS, 512), F32),
         vmem((ROWS, 512), F32), vmem((ROWS, 512), F32), vmem((ROWS, 128), F32),
         vmem((28, 512), F32), vmem((28, 128), F32), vmem((28, 512), F32), vmem((28, 512), F32),
         vmem((PROP, ROWS, 512), F32), vmem((2048, 128), BF16), vmem((2, ROWS, 128), F32),
         vmem((ROWS, 128), F32),
         pltpu.SMEM((SEQ,), jnp.int32),
-        pltpu.SemaphoreType.DMA((21,)),
-        pltpu.SemaphoreType.DMA((10, N)),
-        pltpu.SemaphoreType.DMA((10, N + 2)),
+        pltpu.SemaphoreType.DMA((9,)),
+        pltpu.SemaphoreType.DMA((10,)),
+        pltpu.SemaphoreType.DMA((22,)),
+        pltpu.SemaphoreType.REGULAR,
     ]
     held = pl.pallas_call(
         body,
@@ -458,7 +490,7 @@
         out_shape=[jax.ShapeDtypeStruct(shape, dtype) for shape, dtype in out_shapes],
         in_specs=[pl.BlockSpec(memory_space=vmem)] * 6,
         out_specs=[pl.BlockSpec(memory_space=pl.ANY)] * 6,
-        scratch_shapes=[pltpu.SemaphoreType.DMA((6,))],
+        scratch_shapes=[pltpu.SemaphoreType.DMA((9,))],
         name="finish",
     )(*(pltpu.with_memory_space_constraint(h, vmem) for h in held))
     return (

time: 45.6 us -> 42.8 us (0.939)
  Pallas kernels: 44.8 us -> 42 us
    pallas_call x1, Pallas kernels: 43.8 us -> 40.9 us  [on_device(): pl.pallas_call(body, out_shape=[vmem(shape, dtype) for shape, dtype in ou...]
where the time goes in v4:
time: 42.8 us; the launch traced here: 42.7 us
  Pallas kernels  42 us (98%)
  between operations  0.65 us (2%)
    pallas_call x1, Pallas kernels, on_device(): pl.pallas_call(body, out_shape=[vmem(shape, dtype) for shape, dtype in ou...  40.9 us
    pallas_call x1, Pallas kernels, on_device(): pl.pallas_call(finish, out_shape=[jax.ShapeDtypeStruct(shape, dtype) for...  1.07 us

profile of v4, /device:TPU:1, one launch (start us, length us, event | category | flops | bytes accessed | tf_op | source)
XLA Modules:
  0.0 42.7 jit_solution(2757227601292591296)
XLA Ops:
  0.6 40.9 %mixer.1 = (bf16[4,4,256]{2,1,0:T(4,128)(2,1)S(1)}, f32[2048,128]{1,0:T(8,128)S(1)}, bf16[7,4,512]{2,1,0:T(4,128)(2,1)S(1)}, bf16[7,4,128]{2,1,0:T(4,128)(2,1)S(...) custom-call(bf16[4,4,256]{2,1,0:T(4,128)(2,1)} %tokens.1, f32[1,2048]{1,0:T(1,128)} %bitcast.19, ...), custom_call_target="tpu_custom_call" | custom-call | tf_op jit(solution)/shard_map/mixer/pallas_call | solution.py:479
  41.6 1.1 %finish.1 = (bf16[4,4,256]{2,1,0:T(4,128)(2,1)}, f32[2048,128]{1,0:T(8,128)}, bf16[7,4,512]{2,1,0:T(4,128)(2,1)}, bf16[7,4,128]{2,1,0:T(4,128)(2,1)}, bf16[7,4,1...) custom-call(bf16[4,4,256]{2,1,0:T(4,128)(2,1)S(1)} %get-tuple-element.18.refs_0_, f32[2048,128]{1,0:T(8,128)S(1)} %get-tuple-element.19.refs_1_, ...), custom_call_target="tpu_custom_call" | custom-call | tf_op jit(solution)/shard_map/finish/pallas_call | solution.py:488

commit v5 on v4

--- a/solution.py
+++ b/solution.py
@@ -22,6 +22,7 @@
 ORDER = (4, 3, 5, 2, 6, 1, 7)
 
 T1, T2Y, T2Z, WY, WZ, RSY, RSZ, OW, O1, O2 = range(10)
+LATE = 22
 
 
 def silu(v):
@@ -53,17 +54,17 @@
 ):
     kv = lax.axis_index("kv")
     tp = lax.axis_index("tp")
-    z = kv // N
-    y = kv % N
+    z = lax.div(kv, N)
+    y = lax.rem(kv, N)
 
     def at(rows, count):
         return pl.ds(pl.multiple_of(rows * count, count), count)
 
     def up(d):
-        return z * N + (y + d) % N
+        return z * N + lax.rem(y + d, N)
 
     def over(d):
-        return ((z + d) % N) * N + y
+        return (lax.rem(z + d, N)) * N + y
 
     groups = (
         (
@@ -108,7 +109,7 @@
         pl.semaphore_signal(barrier, inc=1, device_id=(k, t), device_id_type=MESH)
 
     for d in range(1, N):
-        tell(kv, (tp + d) % N)
+        tell(kv, lax.rem(tp + d, N))
     for d in (1, 7, 2, 6):
         tell(up(d), tp)
         tell(over(d), tp)
@@ -157,16 +158,19 @@
                         slot = early(first, h, side) if d in (2, 6) else phase
                         pass_slab(phase, slot, ref, me, h, dev(d))
 
+    def spread_far(rings):
+        for h in range(2):
+            for phase, first, ref, me, dev in rings:
+                pass_slab(phase, phase, ref, me, h, dev(4))
+
     def spread_on(rings):
         for h in range(2):
-            for side, (back_two, one, two) in enumerate(((6, 1, 2), (2, 7, 6))):
+            for side, (back_two, one) in enumerate(((6, 1), (2, 7))):
                 for phase, first, ref, me, dev in rings:
-                    owner = (me + back_two) % N
+                    owner = lax.rem(me + back_two, N)
                     part = slab(ref, owner, h)
                     copy(phase, early(first, h, side), part, part, kv, tp).wait_recv()
                     pass_slab(phase, phase, ref, owner, h, dev(one))
-                    if h == side:
-                        pass_slab(phase, phase, ref, owner, h, dev(two))
 
     def spread_end(ring):
         arrived(ring[0], ring[2].at[pl.ds(0, 160), :])
@@ -176,7 +180,7 @@
     ring_o = (OW, 18, owg, y, up)
 
     for d in range(1, N):
-        send(T1, xall.at[tp], xall.at[tp], kv, (tp + d) % N)
+        send(T1, xall.at[tp], xall.at[tp], kv, lax.rem(tp + d, N))
     spread_own((ring_y, ring_z))
 
     loaded(1, base_m.at[pl.ds(0, 128), :])
@@ -186,6 +190,9 @@
         ppv[SEQ * r : SEQ * r + SEQ, :] = pv_m[r].astype(F32)
         ppb[SEQ * r : SEQ * r + SEQ, :] = pb_m[r].astype(F32)
         ppc[SEQ * r : SEQ * r + SEQ, :] = pc_m[r].astype(F32)
+
+    pl.semaphore_wait(hello, 4)
+    spread_far((ring_y, ring_z))
 
     arrived(T1, xall.at[pl.ds(0, N - 1)])
     blocks = [xall[t].astype(F32) for t in range(N)]
@@ -199,9 +206,8 @@
         nrm[t] = block
         normed.append(block.astype(F32))
     ay[at(z, ROWS), :] = nrm[z]
-    pl.semaphore_wait(hello, 4)
     for d in ORDER:
-        zz = (z + d) % N
+        zz = lax.rem(z + d, N)
         send(T2Y, nrm.at[zz], ay.at[at(z, ROWS), :], over(d), tp)
     lane = lax.broadcasted_iota(jnp.int32, (ROWS, 128), 1) // 32
     for yy in range(N):
@@ -217,7 +223,7 @@
             npk[yy, :, 128 * half : 128 * half + 128] = tile.astype(BF16)
     az[at(y, ROWS), :] = npk[y]
     for d in ORDER:
-        yy = (y + d) % N
+        yy = lax.rem(y + d, N)
         send(T2Z, npk.at[yy], az.at[at(y, ROWS), :], up(d), tp)
     spread_on((ring_y, ring_z))
 
@@ -307,16 +313,38 @@
     window(ppc, rrc, 128)
 
     rest = pl.ds(0, ROWS * (N - 1))
-    arrived(T2Y, ay.at[rest, :])
-    arrived(T2Z, az.at[rest, :])
-    spread_end(ring_y)
-    py[...] = jnp.dot(ay[...], wy[...], preferred_element_type=F32).astype(BF16)
-    spread_end(ring_z)
-    pz[...] = jnp.dot(az[...], wz[...], preferred_element_type=F32).astype(BF16)
-    for d in ORDER:
-        zz, yy = (z + d) % N, (y + d) % N
-        send(RSY, py.at[at(zz, ROWS), :], rsy.at[z], over(d), tp)
-        send(RSZ, pz.at[at(yy, ROWS), :], rsz.at[y], up(d), tp)
+
+    def others(me):
+        return [i + jnp.where(me <= i, 1, 0).astype(jnp.int32) for i in range(N - 1)]
+
+    def sums_y():
+        arrived(T2Z, az.at[rest, :])
+        spread_end(ring_z)
+        pz[...] = jnp.dot(az[...], wz[...], preferred_element_type=F32).astype(BF16)
+        for yy in others(y):
+            send(RSZ, pz.at[at(yy, ROWS), :], rsz.at[y], z * N + yy, tp)
+
+    def sums_z():
+        arrived(T2Y, ay.at[rest, :])
+        spread_end(ring_y)
+        py[...] = jnp.dot(ay[...], wy[...], preferred_element_type=F32).astype(BF16)
+        for zz in others(z):
+            send(RSY, py.at[at(zz, ROWS), :], rsy.at[z], zz * N + y, tp)
+
+    @pl.when(z < 4)
+    def _():
+        sums_y()
+        sums_z()
+        spread_own((ring_o,))
+        spread_far((ring_o,))
+
+    @pl.when(z >= 4)
+    def _():
+        sums_z()
+        spread_own((ring_o,))
+        spread_far((ring_o,))
+        sums_y()
+
     rsy[z] = py[at(z, ROWS), :]
     rsz[y] = pz[at(y, ROWS), :]
 
@@ -331,7 +359,9 @@
             root_m[lo : lo + 64, :] = new
             rootb[lo : lo + 64, :] = new.astype(BF16)
 
-    spread_own((ring_o,))
+    @pl.when(z >= 4)
+    def _():
+        spread_on((ring_o,))
 
     arrived(RSY, rsy.at[pl.ds(0, N - 1)])
     arrived(RSZ, rsz.at[pl.ds(0, N - 1)])
@@ -366,9 +396,13 @@
     g = out * silu(gate)
     g = g * lax.rsqrt(jnp.mean(g * g, axis=-1, keepdims=True) + EPSILON)
     nrg[at(z, ROWS), :] = (g * og_m[...]).astype(BF16)
+    slot = LATE + lax.div(z, 2)
     for d in ORDER:
-        send(O1, nrg.at[at(z, ROWS), :], nrg.at[at(z, ROWS), :], over(d), tp)
-    spread_on((ring_o,))
+        copy(O1, slot, nrg.at[at(z, ROWS), :], nrg.at[at(z, ROWS), :], over(d), tp).start()
+
+    @pl.when(z < 4)
+    def _():
+        spread_on((ring_o,))
 
     for r in range(PAST):
         nv_m[r] = rrv[SEQ * r : SEQ * r + SEQ, :].astype(BF16)
@@ -376,24 +410,41 @@
         nc_m[r] = rrc[SEQ * r : SEQ * r + SEQ, :].astype(BF16)
 
     spread_end(ring_o)
-    arrived(O1, nrg.at[rest, :])
-    po[...] = lax.dot_general(nrg[...], owg[...], NT, preferred_element_type=F32).astype(BF16)
-
-    def back(d):
-        zz = (z + d) % N
-        send(O2, po.at[at(zz, ROWS), :], osum.at[tp], over(d), z)
-
-    for d in ORDER:
-        back(d)
+    for pair in range(4):
+        near = lax.div(z, 2) == pair
+        sem = LATE + pair
+
+        @pl.when(near)
+        def _():
+            one = nrg.at[pl.ds(0, ROWS), :]
+            copy(O1, sem, one, one, kv, tp).wait_recv()
+
+        @pl.when(jnp.logical_not(near))
+        def _():
+            two = nrg.at[pl.ds(0, 2 * ROWS), :]
+            copy(O1, sem, two, two, kv, tp).wait_recv()
+
+        part = pl.ds(32 * pair, 32)
+        po[part, :] = lax.dot_general(
+            nrg[part, :], owg[...], NT, preferred_element_type=F32
+        ).astype(BF16)
+        for zz in (2 * pair, 2 * pair + 1):
+            local = jnp.logical_and(z == zz, tp == zz)
+
+            @pl.when(jnp.logical_not(local))
+            def _():
+                send(O2, po.at[pl.ds(ROWS * zz, ROWS), :], osum.at[tp], zz * N + y, z)
+
+            @pl.when(local)
+            def _():
+                osum[tp] = po[ROWS * zz : ROWS * zz + ROWS, :]
 
     @pl.when(z != tp)
     def _():
-        back(0)
         arrived(O2, osum)
 
     @pl.when(z == tp)
     def _():
-        osum[tp] = po[at(z, ROWS), :]
         arrived(O2, osum.at[pl.ds(0, N - 1)])
 
     total = osum[0].astype(F32)
@@ -473,7 +524,7 @@
         pltpu.SMEM((SEQ,), jnp.int32),
         pltpu.SemaphoreType.DMA((9,)),
         pltpu.SemaphoreType.DMA((10,)),
-        pltpu.SemaphoreType.DMA((22,)),
+        pltpu.SemaphoreType.DMA((26,)),
         pltpu.SemaphoreType.REGULAR,
     ]
     held = pl.pallas_call(

time: 42.8 us -> 41.9 us (0.979)
  Pallas kernels: 42 us -> 41.1 us
    pallas_call x1, Pallas kernels: 40.9 us -> 40 us  [on_device(): pl.pallas_call(body, out_shape=[vmem(shape, dtype) for shape, dtype in ou...]
where the time goes in v5:
time: 41.9 us; the launch traced here: 41.7 us
  Pallas kernels  41.1 us (98%)
  between operations  0.65 us (2%)
    pallas_call x1, Pallas kernels, on_device(): pl.pallas_call(body, out_shape=[vmem(shape, dtype) for shape, dtype in ou...  40 us
    pallas_call x1, Pallas kernels, on_device(): pl.pallas_call(finish, out_shape=[jax.ShapeDtypeStruct(shape, dtype) for...  1.07 us

profile of v5, /device:TPU:1, one launch (start us, length us, event | category | flops | bytes accessed | tf_op | source)
XLA Modules:
  0.0 41.7 jit_solution(6129995529707012037)
XLA Ops:
  0.6 40.0 %mixer.1 = (bf16[4,4,256]{2,1,0:T(4,128)(2,1)S(1)}, f32[2048,128]{1,0:T(8,128)S(1)}, bf16[7,4,512]{2,1,0:T(4,128)(2,1)S(1)}, bf16[7,4,128]{2,1,0:T(4,128)(2,1)S(...) custom-call(bf16[4,4,256]{2,1,0:T(4,128)(2,1)} %tokens.1, f32[1,2048]{1,0:T(1,128)} %bitcast.19, ...), custom_call_target="tpu_custom_call" | custom-call | tf_op jit(solution)/shard_map/mixer/pallas_call | solution.py:530
  40.6 1.1 %finish.1 = (bf16[4,4,256]{2,1,0:T(4,128)(2,1)}, f32[2048,128]{1,0:T(8,128)}, bf16[7,4,512]{2,1,0:T(4,128)(2,1)}, bf16[7,4,128]{2,1,0:T(4,128)(2,1)}, bf16[7,4,1...) custom-call(bf16[4,4,256]{2,1,0:T(4,128)(2,1)S(1)} %get-tuple-element.18.refs_0_, f32[2048,128]{1,0:T(8,128)S(1)} %get-tuple-element.19.refs_1_, ...), custom_call_target="tpu_custom_call" | custom-call | tf_op jit(solution)/shard_map/finish/pallas_call | solution.py:539

commit v6 on v5

--- a/solution.py
+++ b/solution.py
@@ -128,7 +128,8 @@
 
     def copy(phase, slot, src, dst, k, t):
         return pltpu.make_async_remote_copy(
-            src_ref=src, dst_ref=dst, send_sem=send_sem.at[phase], recv_sem=recv_sem.at[slot],
+            src_ref=src, dst_ref=dst, send_sem=send_sem.at[1 if phase in (OW, O1, O2) else 0],
+            recv_sem=recv_sem.at[slot],
             device_id=(k, t), device_id_type=MESH,
         )
 
@@ -150,8 +151,8 @@
     def early(first, h, side):
         return first + 2 * h + side
 
-    def spread_own(rings):
-        for ds in ((2, 6), (1, 7)):
+    def spread_own(rings, steps=((2, 6), (1, 7))):
+        for ds in steps:
             for h in range(2):
                 for side, d in enumerate(ds):
                     for phase, first, ref, me, dev in rings:
@@ -226,6 +227,7 @@
         yy = lax.rem(y + d, N)
         send(T2Z, npk.at[yy], az.at[at(y, ROWS), :], up(d), tp)
     spread_on((ring_y, ring_z))
+    spread_own((ring_o,), ((2, 6),))
 
     head = lax.broadcasted_iota(jnp.int32, (1, 512), 1) // 64
 
@@ -322,7 +324,7 @@
         spread_end(ring_z)
         pz[...] = jnp.dot(az[...], wz[...], preferred_element_type=F32).astype(BF16)
         for yy in others(y):
-            send(RSZ, pz.at[at(yy, ROWS), :], rsz.at[y], z * N + yy, tp)
+            copy(RSZ, RSY, pz.at[at(yy, ROWS), :], rsz.at[y], z * N + yy, tp).start()
 
     def sums_z():
         arrived(T2Y, ay.at[rest, :])
@@ -334,16 +336,16 @@
     @pl.when(z < 4)
     def _():
         sums_y()
+        spread_own((ring_o,), ((1, 7),))
+        spread_far((ring_o,))
         sums_z()
-        spread_own((ring_o,))
-        spread_far((ring_o,))
 
     @pl.when(z >= 4)
     def _():
         sums_z()
-        spread_own((ring_o,))
+        sums_y()
+        spread_own((ring_o,), ((1, 7),))
         spread_far((ring_o,))
-        sums_y()
 
     rsy[z] = py[at(z, ROWS), :]
     rsz[y] = pz[at(y, ROWS), :]
@@ -359,12 +361,9 @@
             root_m[lo : lo + 64, :] = new
             rootb[lo : lo + 64, :] = new.astype(BF16)
 
-    @pl.when(z >= 4)
-    def _():
-        spread_on((ring_o,))
-
-    arrived(RSY, rsy.at[pl.ds(0, N - 1)])
-    arrived(RSZ, rsz.at[pl.ds(0, N - 1)])
+    spread_on((ring_o,))
+
+    arrived(RSY, wy.at[pl.ds(0, 224), :])
 
     def summed(ref, lo, hi):
         total = ref[0, :, lo:hi].astype(F32)
@@ -396,39 +395,39 @@
     g = out * silu(gate)
     g = g * lax.rsqrt(jnp.mean(g * g, axis=-1, keepdims=True) + EPSILON)
     nrg[at(z, ROWS), :] = (g * og_m[...]).astype(BF16)
-    slot = LATE + lax.div(z, 2)
+    slot = LATE + jnp.where(z < 2, z, lax.div(z, 2) + 1).astype(jnp.int32)
     for d in ORDER:
         copy(O1, slot, nrg.at[at(z, ROWS), :], nrg.at[at(z, ROWS), :], over(d), tp).start()
-
-    @pl.when(z < 4)
-    def _():
-        spread_on((ring_o,))
-
     for r in range(PAST):
         nv_m[r] = rrv[SEQ * r : SEQ * r + SEQ, :].astype(BF16)
         nb_m[r] = rrb[SEQ * r : SEQ * r + SEQ, :].astype(BF16)
         nc_m[r] = rrc[SEQ * r : SEQ * r + SEQ, :].astype(BF16)
 
     spread_end(ring_o)
-    for pair in range(4):
-        near = lax.div(z, 2) == pair
-        sem = LATE + pair
-
-        @pl.when(near)
+    for i, (low, high) in enumerate(((0, 1), (1, 2), (2, 4), (4, 6), (6, 8))):
+        mine = jnp.logical_and(z >= low, z < high)
+        sem = LATE + i
+
+        def landed(count):
+            if count:
+                some = nrg.at[pl.ds(0, count * ROWS), :]
+                copy(O1, sem, some, some, kv, tp).wait_recv()
+
+        if high - low > 1:
+
+            @pl.when(mine)
+            def _():
+                landed(high - low - 1)
+
+        @pl.when(jnp.logical_not(mine))
         def _():
-            one = nrg.at[pl.ds(0, ROWS), :]
-            copy(O1, sem, one, one, kv, tp).wait_recv()
-
-        @pl.when(jnp.logical_not(near))
-        def _():
-            two = nrg.at[pl.ds(0, 2 * ROWS), :]
-            copy(O1, sem, two, two, kv, tp).wait_recv()
-
-        part = pl.ds(32 * pair, 32)
+            landed(high - low)
+
+        part = pl.ds(ROWS * low, ROWS * (high - low))
         po[part, :] = lax.dot_general(
             nrg[part, :], owg[...], NT, preferred_element_type=F32
         ).astype(BF16)
-        for zz in (2 * pair, 2 * pair + 1):
+        for zz in range(low, high):
             local = jnp.logical_and(z == zz, tp == zz)
 
             @pl.when(jnp.logical_not(local))
@@ -457,23 +456,15 @@
                 pl.ds(q, PROP, stride=SEQ), :
             ].astype(BF16)
 
-    gone(T1, xall.at[pl.ds(0, N - 1)])
-    gone(T2Y, ay.at[rest, :])
-    gone(T2Z, az.at[rest, :])
-    gone(WY, wy.at[pl.ds(0, 224), :])
-    gone(WZ, wz.at[pl.ds(0, 224), :])
-    gone(RSY, rsy.at[pl.ds(0, N - 1)])
-    gone(RSZ, rsz.at[pl.ds(0, N - 1)])
-    gone(OW, owg.at[pl.ds(0, 224), :])
-    gone(O1, nrg.at[rest, :])
+    gone(T1, base_m.at[pl.ds(0, 2016), :])
 
     @pl.when(z != tp)
     def _():
-        gone(O2, osum)
+        gone(O2, base_m.at[pl.ds(0, 800), :])
 
     @pl.when(z == tp)
     def _():
-        gone(O2, osum.at[pl.ds(0, N - 1)])
+        gone(O2, base_m.at[pl.ds(0, 784), :])
 
 
 def finish(*refs):
@@ -523,8 +514,8 @@
         vmem((ROWS, 128), F32),
         pltpu.SMEM((SEQ,), jnp.int32),
         pltpu.SemaphoreType.DMA((9,)),
-        pltpu.SemaphoreType.DMA((10,)),
-        pltpu.SemaphoreType.DMA((26,)),
+        pltpu.SemaphoreType.DMA((2,)),
+        pltpu.SemaphoreType.DMA((27,)),
         pltpu.SemaphoreType.REGULAR,
     ]
     held = pl.pallas_call(

time: 41.9 us -> 41.7 us (level)
  the two profiles are of different devices: /device:TPU:1 before, /device:TPU:20 now
where the time goes in v6:
time: 41.7 us; the launch traced here: 41.6 us
  Pallas kernels  41 us (98%)
  between operations  0.65 us (2%)
    pallas_call x1, Pallas kernels, on_device(): pl.pallas_call(body, out_shape=[vmem(shape, dtype) for shape, dtype in ou...  39.9 us
    pallas_call x1, Pallas kernels, on_device(): pl.pallas_call(finish, out_shape=[jax.ShapeDtypeStruct(shape, dtype) for...  1.07 us

profile of v6, /device:TPU:20, one launch (start us, length us, event | category | flops | bytes accessed | tf_op | source)
XLA Modules:
  0.0 41.6 jit_solution(3928423392515253717)
XLA Ops:
  0.6 39.9 %mixer.1 = (bf16[4,4,256]{2,1,0:T(4,128)(2,1)S(1)}, f32[2048,128]{1,0:T(8,128)S(1)}, bf16[7,4,512]{2,1,0:T(4,128)(2,1)S(1)}, bf16[7,4,128]{2,1,0:T(4,128)(2,1)S(...) custom-call(bf16[4,4,256]{2,1,0:T(4,128)(2,1)} %tokens.1, f32[1,2048]{1,0:T(1,128)} %bitcast.19, ...), custom_call_target="tpu_custom_call" | custom-call | tf_op jit(solution)/shard_map/mixer/pallas_call | solution.py:521
  40.5 1.1 %finish.1 = (bf16[4,4,256]{2,1,0:T(4,128)(2,1)}, f32[2048,128]{1,0:T(8,128)}, bf16[7,4,512]{2,1,0:T(4,128)(2,1)}, bf16[7,4,128]{2,1,0:T(4,128)(2,1)}, bf16[7,4,1...) custom-call(bf16[4,4,256]{2,1,0:T(4,128)(2,1)S(1)} %get-tuple-element.18.refs_0_, f32[2048,128]{1,0:T(8,128)S(1)} %get-tuple-element.19.refs_1_, ...), custom_call_target="tpu_custom_call" | custom-call | tf_op jit(solution)/shard_map/finish/pallas_call | solution.py:530

commit v7 on v6

--- a/solution.py
+++ b/solution.py
@@ -84,13 +84,13 @@
             (conv_b, cb_m),
             (conv_c, cc_m),
             (output_gain, og_m),
+            (step_w, stepw_m),
         ),
         ((past_s, ps_m),),
         ((step_bias, bias_m),),
         ((decay_log, decay_m),),
         ((skip_gain, skip_m),),
         ((accepted, taken_m),),
-        ((step_w, stepw_m),),
         ((base, base_m),),
     )
     for i, group in enumerate(groups):
@@ -184,8 +184,8 @@
         send(T1, xall.at[tp], xall.at[tp], kv, lax.rem(tp + d, N))
     spread_own((ring_y, ring_z))
 
-    loaded(1, base_m.at[pl.ds(0, 128), :])
-    for i in range(2, 9):
+    loaded(1, root_m.at[pl.ds(0, 640), :])
+    for i in range(2, 8):
         loaded(i)
     for r in range(PAST):
         ppv[SEQ * r : SEQ * r + SEQ, :] = pv_m[r].astype(F32)
@@ -469,8 +469,9 @@
 
 def finish(*refs):
     ins, outs, sem = refs[:6], refs[6:12], refs[12]
-    pairs = [(s, d) for i, (s, d) in enumerate(zip(ins, outs)) if i != 1]
-    pairs += [(ins[1].at[part], outs[1].at[part]) for part in (pl.ds(512 * i, 512) for i in range(4))]
+    parts = [pl.ds(256 * i, 256) for i in range(8)]
+    pairs = [(ins[1].at[part], outs[1].at[part]) for part in parts]
+    pairs += [(s, d) for i, (s, d) in enumerate(zip(ins, outs)) if i != 1]
     copies = [pltpu.make_async_copy(s, d, sem.at[i]) for i, (s, d) in enumerate(pairs)]
     for c in copies:
         c.start()
@@ -513,7 +514,7 @@
         vmem((PROP, ROWS, 512), F32), vmem((2048, 128), BF16), vmem((2, ROWS, 128), F32),
         vmem((ROWS, 128), F32),
         pltpu.SMEM((SEQ,), jnp.int32),
-        pltpu.SemaphoreType.DMA((9,)),
+        pltpu.SemaphoreType.DMA((8,)),
         pltpu.SemaphoreType.DMA((2,)),
         pltpu.SemaphoreType.DMA((27,)),
         pltpu.SemaphoreType.REGULAR,
@@ -532,7 +533,7 @@
         out_shape=[jax.ShapeDtypeStruct(shape, dtype) for shape, dtype in out_shapes],
         in_specs=[pl.BlockSpec(memory_space=vmem)] * 6,
         out_specs=[pl.BlockSpec(memory_space=pl.ANY)] * 6,
-        scratch_shapes=[pltpu.SemaphoreType.DMA((9,))],
+        scratch_shapes=[pltpu.SemaphoreType.DMA((13,))],
         name="finish",
     )(*(pltpu.with_memory_space_constraint(h, vmem) for h in held))
     return (

time: 41.7 us -> 41.7 us (level)
  no operation moved by 1% of the time
where the time goes in v7:
time: 41.7 us; the launch traced here: 41.6 us
  Pallas kernels  41 us (98%)
  between operations  0.65 us (2%)
    pallas_call x1, Pallas kernels, on_device(): pl.pallas_call(body, out_shape=[vmem(shape, dtype) for shape, dtype in ou...  39.9 us
    pallas_call x1, Pallas kernels, on_device(): pl.pallas_call(finish, out_shape=[jax.ShapeDtypeStruct(shape, dtype) for...  1.08 us

profile of v7, /device:TPU:20, one launch (start us, length us, event | category | flops | bytes accessed | tf_op | source)
XLA Modules:
  0.0 41.6 jit_solution(9216327748165256703)
XLA Ops:
  0.6 39.9 %mixer.1 = (bf16[4,4,256]{2,1,0:T(4,128)(2,1)S(1)}, f32[2048,128]{1,0:T(8,128)S(1)}, bf16[7,4,512]{2,1,0:T(4,128)(2,1)S(1)}, bf16[7,4,128]{2,1,0:T(4,128)(2,1)S(...) custom-call(bf16[4,4,256]{2,1,0:T(4,128)(2,1)} %tokens.1, f32[1,2048]{1,0:T(1,128)} %bitcast.19, ...), custom_call_target="tpu_custom_call" | custom-call | tf_op jit(solution)/shard_map/mixer/pallas_call | solution.py:522
  40.5 1.1 %finish.1 = (bf16[4,4,256]{2,1,0:T(4,128)(2,1)}, f32[2048,128]{1,0:T(8,128)}, bf16[7,4,512]{2,1,0:T(4,128)(2,1)}, bf16[7,4,128]{2,1,0:T(4,128)(2,1)}, bf16[7,4,1...) custom-call(bf16[4,4,256]{2,1,0:T(4,128)(2,1)S(1)} %get-tuple-element.18.refs_0_, f32[2048,128]{1,0:T(8,128)S(1)} %get-tuple-element.19.refs_1_, ...), custom_call_target="tpu_custom_call" | custom-call | tf_op jit(solution)/shard_map/finish/pallas_call | solution.py:531
